TPU v7x, 512 devices: a whole 4x4x16 slice. The times are simulated.
512 devices in a mesh: gr: 2 (over z_hi), fs: 32 (over z_lo, y), tp: 8 (over x, core).
Axes of the slice: x: 4, y: 4, z: 16 (z_hi: 2, z_lo: 8; z = z_hi * 8 + z_lo), core: 2. Of those that a mesh axis runs over, the one named last changes fastest.
Arguments:
- prompt: bfloat16 [8192, 2048], P(('gr', 'tp'), 'fs'), may hold values from -2.5 to 2.5
- gain_pre: float32 [2048], P(('gr', 'fs')), may hold values from 0.1 to 1.9
- gate_pre: float32 [2048, 5632], P(('gr', 'fs'), 'tp'), may hold values from -6 to 6
- up_pre: float32 [2048, 5632], P(('gr', 'fs'), 'tp'), may hold values from -6 to 6
- down_pre: float32 [2048, 5632], P(('gr', 'fs'), 'tp'), may hold values from -16 to 16
- gain_post: float32 [2048], P(('gr', 'fs')), may hold values from 0.1 to 1.9
- gate_post: float32 [2048, 5632], P(('gr', 'fs'), 'tp'), may hold values from -6 to 6
- up_post: float32 [2048, 5632], P(('gr', 'fs'), 'tp'), may hold values from -6 to 6
- down_post: float32 [2048, 5632], P(('gr', 'fs'), 'tp'), may hold values from -16 to 16
Outputs:
- result: bfloat16 [8192, 2048], P(('gr', 'tp'), 'fs')
- gate_first: bfloat16 [5632, 2048], P('fs')
- up_first: bfloat16 [5632, 2048], P('fs')
- down_first: bfloat16 [5632, 2048], P('fs')
- gate_second: bfloat16 [5632, 2048], P('fs')
- up_second: bfloat16 [5632, 2048], P('fs')
- down_second: bfloat16 [5632, 2048], P('fs')
All inputs are finite; a program needn't handle non-finite values.
Results may differ from a plain program's by a relative error of at most 0.028.
Values may be sent and summed in bfloat16 or wider, within the bound.
A program may use at most 64 MiB of HBM per device.

v0:
```python
import jax
import jax.numpy as jnp
from jax import lax
from jax.sharding import PartitionSpec as P

D = 2048
FF = 5632


norm_eps = 1e-06


def copy_for_each(shard, axis):
    copies = jnp.broadcast_to(shard, (lax.axis_size(axis), *shard.shape))
    return lax.all_to_all(copies, axis, split_axis=0, concat_axis=0, tiled=True)


def laid_out(blocks, dim):
    dims = list(blocks.shape[1:])
    dims[dim] *= blocks.shape[0]
    return jnp.moveaxis(blocks, 0, dim).reshape(dims)


def gathered_copies(shard, axis, dim):
    blocks = copy_for_each(shard, axis)
    return laid_out(blocks, dim)


def in_blocks(shard, dim, size):
    dims = shard.shape
    blocks = shard.reshape(*dims[:dim], size, dims[dim] // size, *dims[dim + 1 :])
    return jnp.moveaxis(blocks, dim, 0)


def summed_on_arrival(shard, axis, dim):
    size = lax.axis_size(axis)
    blocks = lax.all_to_all(in_blocks(shard, dim, size), axis, 0, 0, tiled=True)
    return jnp.sum(blocks.astype(jnp.float32), axis=0)


def in_one_piece(arrays, axis, dim, along):
    ends, at = ([], 0)
    for a in arrays[:-1]:
        at += a.shape[along]
        ends.append(at)
    both = jnp.concatenate(arrays, axis=along)
    return tuple(jnp.split(lax.all_gather(both, axis, axis=dim, tiled=True), ends, axis=along))


def add_products(columns_in, w_gate, w_up):
    widened = columns_in.astype(jnp.float32)
    dims = (((1,), (1,)), ((), ()))
    return (
        lax.dot_general(columns_in, w_gate, dims, preferred_element_type=jnp.float32),
        lax.dot_general(columns_in, w_up, dims, preferred_element_type=jnp.float32),
        jnp.sum(widened * widened, axis=1),
    )


def half_step(tokens, w_gate, w_up, w_down):
    gate_sum, up_sum, squares = add_products(gathered_copies(tokens, "fs", 1), w_gate, w_up)
    row_scale = (lax.rsqrt(squares / D + norm_eps) * D ** (-0.5))[:, None]
    hidden = (jax.nn.silu(gate_sum * row_scale) * (up_sum * row_scale)).astype(jnp.bfloat16)
    partial_value = jnp.dot(hidden, w_down, preferred_element_type=jnp.float32)
    summed = summed_on_arrival(partial_value.astype(jnp.bfloat16), "fs", 1)
    return (tokens.astype(jnp.float32) + 0.5 * FF ** (-0.5) * summed).astype(jnp.bfloat16)


def restore_rows(matrix, groups, shards, lanes):
    row_total, col_total = matrix.shape
    sub_rows = row_total // (groups * shards * lanes)
    shaped = matrix.reshape(groups, lanes, shards, sub_rows, col_total)
    return jnp.transpose(shaped, (0, 2, 1, 3, 4)).reshape(row_total, col_total)


def relayout(matrices):
    crossed = (
        lax.all_to_all(
            lax.all_to_all(matrices[0], "tp", split_axis=0, concat_axis=1, tiled=True),
            "fs",
            split_axis=1,
            concat_axis=0,
            tiled=True,
        ),
        lax.all_to_all(
            lax.all_to_all(matrices[1], "tp", split_axis=0, concat_axis=1, tiled=True),
            "fs",
            split_axis=1,
            concat_axis=0,
            tiled=True,
        ),
        lax.all_to_all(
            lax.all_to_all(matrices[2], "tp", split_axis=0, concat_axis=1, tiled=True),
            "fs",
            split_axis=1,
            concat_axis=0,
            tiled=True,
        ),
        lax.all_to_all(
            lax.all_to_all(matrices[3], "tp", split_axis=0, concat_axis=1, tiled=True),
            "fs",
            split_axis=1,
            concat_axis=0,
            tiled=True,
        ),
        lax.all_to_all(
            lax.all_to_all(matrices[4], "tp", split_axis=0, concat_axis=1, tiled=True),
            "fs",
            split_axis=1,
            concat_axis=0,
            tiled=True,
        ),
        lax.all_to_all(
            lax.all_to_all(matrices[5], "tp", split_axis=0, concat_axis=1, tiled=True),
            "fs",
            split_axis=1,
            concat_axis=0,
            tiled=True,
        ),
    )
    gathered = in_one_piece(
        (crossed[0], crossed[1], crossed[2], crossed[3], crossed[4], crossed[5]), ("gr", "tp"), 0, 1
    )
    groups = lax.axis_size("gr")
    shards = lax.axis_size("fs")
    lanes = lax.axis_size("tp")
    return tuple((restore_rows(matrix, groups, shards, lanes).T for matrix in gathered))


def local(prompt, gain_pre, gate_pre, up_pre, down_pre, gain_post, gate_post, up_post, down_post):
    rounded = (
        (gain_pre[:, None] * gate_pre).astype(jnp.bfloat16),
        (gain_pre[:, None] * up_pre).astype(jnp.bfloat16),
        down_pre.astype(jnp.bfloat16),
        (gain_post[:, None] * gate_post).astype(jnp.bfloat16),
        (gain_post[:, None] * up_post).astype(jnp.bfloat16),
        down_post.astype(jnp.bfloat16),
    )
    served = relayout(rounded)
    middle = half_step(prompt, served[0], served[1], served[2])
    result = half_step(middle, served[3], served[4], served[5])
    return (result, served[0], served[1], served[2], served[3], served[4], served[5])


def solution(mesh):
    placed = (
        P(("gr", "tp"), "fs"),
        P(("gr", "fs")),
        P(("gr", "fs"), "tp"),
        P(("gr", "fs"), "tp"),
        P(("gr", "fs"), "tp"),
        P(("gr", "fs")),
        P(("gr", "fs"), "tp"),
        P(("gr", "fs"), "tp"),
        P(("gr", "fs"), "tp"),
    )
    return jax.shard_map(
        local,
        mesh=mesh,
        in_specs=placed,
        out_specs=(
            P(("gr", "tp"), "fs"),
            P("fs", None),
            P("fs", None),
            P("fs", None),
            P("fs", None),
            P("fs", None),
            P("fs", None),
        ),
        check_vma=False,
    )
```

profile of v0, /device:TPU:6, one launch (start us, length us, event | category | flops | bytes accessed | tf_op | source)
XLA Modules:
  0.0 711.1 jit_solution(13463120241691673238)
XLA Ops:
  8.8 9.1 %all-to-all-start = ((bf16[8,4,704]{2,1,0:T(4,128)(2,1)}), bf16[8,4,704]{2,1,0:T(4,128)(2,1)S(1)}, u32[]{:S(2)}, u32[]{:S(2)}) async-start(bf16[8,4,704]{2,1,0:T(4,128)(2,1)} %all_to_all.168), calls=%async_computation | async-start | bytes 98304 | tf_op jit(solution)/shard_map/all_to_all | solution.py:79
  18.6 2.8 all-to-all-done
  21.4 5.4 all-to-all-start.2
  30.2 5.4 all-to-all-start.6
  36.2 2.8 all-to-all-done.6
  39.0 5.4 all-to-all-start.8
  47.8 5.4 all-to-all-start.4
  56.6 5.4 all-to-all-start.10
  65.4 11.2 %all-to-all-start.1 = ((bf16[4,32,176]{2,0,1:T(4,128)(2,1)}), bf16[4,32,176]{2,0,1:T(4,128)(2,1)S(1)}, u32[]{:S(2)}, u32[]{:S(2)}) async-start(bf16[4,32,176]{2,0,1:T(4,128)(2,1)} %copy.45), calls=%async_computation.1 | async-start | bytes 131072 | tf_op jit(solution)/shard_map/all_to_all | solution.py:78
  77.5 12.0 %all-to-all-done.1 = bf16[4,32,176]{2,0,1:T(4,128)(2,1)S(1)} async-done(((bf16[4,32,176]{2,0,1:T(4,128)(2,1)}), bf16[4,32,176]{2,0,1:T(4,128)(2,1)S(1)}, u32[]{:S(2)}, u32[]{:S(2)}) %all-to-all-start.1) | async-done | bytes 45088 | tf_op jit(solution)/shard_map/all_to_all | solution.py:78
  89.5 3.9 all-to-all-start.3
  94.2 12.0 %all-to-all-done.3 = bf16[4,32,176]{2,0,1:T(4,128)(2,1)S(1)} async-done(((bf16[4,32,176]{2,0,1:T(4,128)(2,1)}), bf16[4,32,176]{2,0,1:T(4,128)(2,1)S(1)}, u32[]{:S(2)}, u32[]{:S(2)}) %all-to-all-start.3) | async-done | bytes 45088 | tf_op jit(solution)/shard_map/all_to_all | solution.py:85
  106.3 3.9 all-to-all-start.7
  111.0 12.0 %all-to-all-done.7 = bf16[4,32,176]{2,0,1:T(4,128)(2,1)S(1)} async-done(((bf16[4,32,176]{2,0,1:T(4,128)(2,1)}), bf16[4,32,176]{2,0,1:T(4,128)(2,1)S(1)}, u32[]{:S(2)}, u32[]{:S(2)}) %all-to-all-start.7) | async-done | bytes 45088 | tf_op jit(solution)/shard_map/all_to_all | solution.py:99
  123.0 3.9 all-to-all-start.9
  127.7 12.0 %all-to-all-done.9 = bf16[4,32,176]{2,0,1:T(4,128)(2,1)S(1)} async-done(((bf16[4,32,176]{2,0,1:T(4,128)(2,1)}), bf16[4,32,176]{2,0,1:T(4,128)(2,1)S(1)}, u32[]{:S(2)}, u32[]{:S(2)}) %all-to-all-start.9) | async-done | bytes 45088 | tf_op jit(solution)/shard_map/all_to_all | solution.py:106
  139.7 3.9 all-to-all-start.5
  143.8 12.7 %all-to-all-done.5 = bf16[4,32,176]{2,0,1:T(4,128)(2,1)S(1)} async-done(((bf16[4,32,176]{2,0,1:T(4,128)(2,1)}), bf16[4,32,176]{2,0,1:T(4,128)(2,1)S(1)}, u32[]{:S(2)}, u32[]{:S(2)}) %all-to-all-start.5) | async-done | bytes 45088 | tf_op jit(solution)/shard_map/all_to_all | solution.py:92
  156.5 16.3 %all_to_all.230 = bf16[4,32,176]{2,0,1:T(4,128)(2,1)S(1)} all-to-all(bf16[4,32,176]{2,0,1:T(4,128)(2,1)S(1)} %copy.55), channel_id=1, replica_groups=mesh['gr'=2,'fs'=32,'tp'=8] {'fs'}, dimensions={1} | all-to-all | bytes 90112 | tf_op jit(solution)/shard_map/all_to_all | solution.py:113
  174.3 4.0 all-to-all-start.12
  179.8 143.7 %all-to-all-done.12 = bf16[32,512,64]{1,2,0:T(8,128)(2,1)S(1)} async-done(((bf16[32,512,64]{1,2,0:T(8,128)(2,1)}), bf16[32,512,64]{1,2,0:T(8,128)(2,1)S(1)}, u32[]{:S(2)}, u32[]{:S(2)}) %all-to-all-start.12) | async-done | bytes 2097184 | tf_op jit(solution)/shard_map/all_to_all | solution.py:15
  324.1 3.1 all-gather.2.cloned.1.call-done
  327.2 8.8 %fusion.22 = (bf16[2048,176]{1,0:T(8,128)(2,1)}, bf16[2048,176]{1,0:T(8,128)(2,1)S(1)}, bf16[2048,176]{1,0:T(8,128)(2,1)}, bf16[2048,176]{1,0:T(8,128)(2,1)}, bf...) fusion(bf16[2048,1056]{1,0:T(8,128)(2,1)} %all-gather.2.cloned.1.call-done), kind=kLoop, calls=%fused_computation.40 | loop fusion | bytes 8650752 | tf_op jit(solution)/shard_map/split | solution.py:47
  360.9 4.3 convolution_convert_fusion.1
  365.2 2.9 copy.59
  368.1 118.8 %all_to_all.231 = bf16[32,512,64]{1,2,0:T(8,128)(2,1)S(1)} all-to-all(bf16[32,512,64]{1,2,0:T(8,128)(2,1)S(1)} %bitcast.63), channel_id=1, replica_groups=mesh['gr'=2,'fs'=32,'tp'=8] {'fs'}, dimensions={0} | all-to-all | bytes 4194304 | tf_op jit(solution)/shard_map/all_to_all | solution.py:37
  488.7 6.6 all-to-all-start.14
  516.7 73.8 %all-to-all-done.14 = bf16[32,512,64]{1,2,0:T(8,128)(2,1)S(1)} async-done(((bf16[32,512,64]{1,2,0:T(8,128)(2,1)}), bf16[32,512,64]{1,2,0:T(8,128)(2,1)S(1)}, u32[]{:S(2)}, u32[]{:S(2)}) %all-to-all-start.14) | async-done | bytes 2097184 | tf_op jit(solution)/shard_map/all_to_all | solution.py:15
  592.4 4.3 convolution_convert_fusion
  596.8 3.9 copy.63
  600.7 7.5 %all-to-all-start.15 = ((bf16[32,512,64]{1,2,0:T(8,128)(2,1)}), bf16[32,512,64]{1,2,0:T(8,128)(2,1)S(1)}, u32[]{:S(2)}, u32[]{:S(2)}) async-start(bf16[32,512,64]{1,2,0:T(8,128)(2,1)} %bitcast.62), calls=%async_computation.15 | async-start | bytes 4194304 | tf_op jit(solution)/shard_map/all_to_all | solution.py:37
  618.5 84.8 %all-to-all-done.15 = bf16[32,512,64]{1,2,0:T(8,128)(2,1)S(1)} async-done(((bf16[32,512,64]{1,2,0:T(8,128)(2,1)}), bf16[32,512,64]{1,2,0:T(8,128)(2,1)S(1)}, u32[]{:S(2)}, u32[]{:S(2)}) %all-to-all-start.15) | async-done | bytes 2097184 | tf_op jit(solution)/shard_map/all_to_all | solution.py:37
  (87 shorter events, 85.1 us)
Async XLA Ops:
  8.8 12.5 %all-to-all-start = ((bf16[8,4,704]{2,1,0:T(4,128)(2,1)}), bf16[8,4,704]{2,1,0:T(4,128)(2,1)S(1)}, u32[]{:S(2)}, u32[]{:S(2)}) async-start(bf16[8,4,704]{2,1,0:T(4,128)(2,1)} %all_to_all.168), calls=%async_computation | async-start | bytes 98304 | tf_op jit(solution)/shard_map/all_to_all | solution.py:79
  21.4 8.8 %all-to-all-start.2 = ((bf16[8,4,704]{2,1,0:T(4,128)(2,1)}), bf16[8,4,704]{2,1,0:T(4,128)(2,1)S(1)}, u32[]{:S(2)}, u32[]{:S(2)}) async-start(bf16[8,4,704]{2,1,0:T(4,128)(2,1)} %all_to_all.175), calls=%async_computation.2 | async-start | bytes 98304 | tf_op jit(solution)/shard_map/all_to_all | solution.py:86
  26.8 146.0 %copy-start.4 = (bf16[512,64]{0,1:T(8,128)(2,1)S(1)}, bf16[512,64]{0,1:T(8,128)(2,1)}, u32[]{:S(2)}) copy-start(bf16[512,64]{0,1:T(8,128)(2,1)} %param.9) | copy-start | bytes 196612
  30.2 8.8 %all-to-all-start.6 = ((bf16[8,4,704]{2,1,0:T(4,128)(2,1)}), bf16[8,4,704]{2,1,0:T(4,128)(2,1)S(1)}, u32[]{:S(2)}, u32[]{:S(2)}) async-start(bf16[8,4,704]{2,1,0:T(4,128)(2,1)} %all_to_all.189), calls=%async_computation.6 | async-start | bytes 98304 | tf_op jit(solution)/shard_map/all_to_all | solution.py:100
  39.0 8.8 %all-to-all-start.8 = ((bf16[8,4,704]{2,1,0:T(4,128)(2,1)}), bf16[8,4,704]{2,1,0:T(4,128)(2,1)S(1)}, u32[]{:S(2)}, u32[]{:S(2)}) async-start(bf16[8,4,704]{2,1,0:T(4,128)(2,1)} %all_to_all.196), calls=%async_computation.8 | async-start | bytes 98304 | tf_op jit(solution)/shard_map/all_to_all | solution.py:107
  47.8 8.8 %all-to-all-start.4 = ((bf16[8,4,704]{2,1,0:T(4,128)(2,1)}), bf16[8,4,704]{2,1,0:T(4,128)(2,1)S(1)}, u32[]{:S(2)}, u32[]{:S(2)}) async-start(bf16[8,4,704]{2,1,0:T(4,128)(2,1)} %all_to_all.182), calls=%async_computation.4 | async-start | bytes 98304 | tf_op jit(solution)/shard_map/all_to_all | solution.py:93
  56.6 8.8 %all-to-all-start.10 = ((bf16[8,4,704]{2,1,0:T(4,128)(2,1)}), bf16[8,4,704]{2,1,0:T(4,128)(2,1)S(1)}, u32[]{:S(2)}, u32[]{:S(2)}) async-start(bf16[8,4,704]{2,1,0:T(4,128)(2,1)} %all_to_all.203), calls=%async_computation.10 | async-start | bytes 98304 | tf_op jit(solution)/shard_map/all_to_all | solution.py:114
  65.4 24.1 %all-to-all-start.1 = ((bf16[4,32,176]{2,0,1:T(4,128)(2,1)}), bf16[4,32,176]{2,0,1:T(4,128)(2,1)S(1)}, u32[]{:S(2)}, u32[]{:S(2)}) async-start(bf16[4,32,176]{2,0,1:T(4,128)(2,1)} %copy.45), calls=%async_computation.1 | async-start | bytes 131072 | tf_op jit(solution)/shard_map/all_to_all | solution.py:78
  89.5 16.7 %all-to-all-start.3 = ((bf16[4,32,176]{2,0,1:T(4,128)(2,1)}), bf16[4,32,176]{2,0,1:T(4,128)(2,1)S(1)}, u32[]{:S(2)}, u32[]{:S(2)}) async-start(bf16[4,32,176]{2,0,1:T(4,128)(2,1)} %copy.47), calls=%async_computation.3 | async-start | bytes 131072 | tf_op jit(solution)/shard_map/all_to_all | solution.py:85
  106.3 16.7 %all-to-all-start.7 = ((bf16[4,32,176]{2,0,1:T(4,128)(2,1)}), bf16[4,32,176]{2,0,1:T(4,128)(2,1)S(1)}, u32[]{:S(2)}, u32[]{:S(2)}) async-start(bf16[4,32,176]{2,0,1:T(4,128)(2,1)} %copy.51), calls=%async_computation.7 | async-start | bytes 131072 | tf_op jit(solution)/shard_map/all_to_all | solution.py:99
  123.0 16.7 %all-to-all-start.9 = ((bf16[4,32,176]{2,0,1:T(4,128)(2,1)}), bf16[4,32,176]{2,0,1:T(4,128)(2,1)S(1)}, u32[]{:S(2)}, u32[]{:S(2)}) async-start(bf16[4,32,176]{2,0,1:T(4,128)(2,1)} %copy.53), calls=%async_computation.9 | async-start | bytes 131072 | tf_op jit(solution)/shard_map/all_to_all | solution.py:106
  139.7 16.7 %all-to-all-start.5 = ((bf16[4,32,176]{2,0,1:T(4,128)(2,1)}), bf16[4,32,176]{2,0,1:T(4,128)(2,1)S(1)}, u32[]{:S(2)}, u32[]{:S(2)}) async-start(bf16[4,32,176]{2,0,1:T(4,128)(2,1)} %copy.49), calls=%async_computation.5 | async-start | bytes 131072 | tf_op jit(solution)/shard_map/all_to_all | solution.py:92
  174.3 149.2 %all-to-all-start.12 = ((bf16[32,512,64]{1,2,0:T(8,128)(2,1)}), bf16[32,512,64]{1,2,0:T(8,128)(2,1)S(1)}, u32[]{:S(2)}, u32[]{:S(2)}) async-start(bf16[32,512,64]{1,2,0:T(8,128)(2,1)} %broadcast_in_dim.4), calls=%async_computation.12 | async-start | bytes 4194304 | tf_op jit(solution)/shard_map/all_to_all | solution.py:15
  178.4 148.8 %all-gather.2.cloned.1.call-start = ((), (), s32[]{:S(2)}) async-start(), calls=%async_computation.16 | async-start | bytes 5013504 | tf_op jit(solution)/shard_map/all_gather | solution.py:47
  488.7 101.8 %all-to-all-start.14 = ((bf16[32,512,64]{1,2,0:T(8,128)(2,1)}), bf16[32,512,64]{1,2,0:T(8,128)(2,1)S(1)}, u32[]{:S(2)}, u32[]{:S(2)}) async-start(bf16[32,512,64]{1,2,0:T(8,128)(2,1)} %broadcast_in_dim.5), calls=%async_computation.14 | async-start | bytes 4194304 | tf_op jit(solution)/shard_map/all_to_all | solution.py:15
  514.1 77.0 %copy-start.2 = (bf16[2048,176]{1,0:T(8,128)(2,1)S(1)}, bf16[2048,176]{1,0:T(8,128)(2,1)}, u32[]{:S(2)}) copy-start(bf16[2048,176]{1,0:T(8,128)(2,1)} %reshape.128) | copy-start | bytes 2162692
  600.7 7.5 %copy-start = (bf16[2048,176]{1,0:T(8,128)(2,1)S(1)}, bf16[2048,176]{1,0:T(8,128)(2,1)}, u32[]{:S(2)}) copy-start(bf16[2048,176]{1,0:T(8,128)(2,1)} %reshape.119) | copy-start | bytes 2162692
  600.7 102.6 %all-to-all-start.15 = ((bf16[32,512,64]{1,2,0:T(8,128)(2,1)}), bf16[32,512,64]{1,2,0:T(8,128)(2,1)S(1)}, u32[]{:S(2)}, u32[]{:S(2)}) async-start(bf16[32,512,64]{1,2,0:T(8,128)(2,1)} %bitcast.62), calls=%async_computation.15 | async-start | bytes 4194304 | tf_op jit(solution)/shard_map/all_to_all | solution.py:37
  609.4 2.3 copy-start.1
  612.9 2.3 copy-start.3
Sparse Core Ops, SparseCore 0:
  183.0 144.0 all-gather.1
where the time goes:
time: 713 us; the launch traced here: 711 us
  waiting for transfers between devices  380 us (53%)
  blocking collectives  135 us (19%)
  local copies, waits for them, and re-layouts  82.1 us (12%)
  starting transfers between devices  80.9 us (11%)
  between operations  14.3 us (2%)
  matrix products  12.5 us (2%)
    all_to_all x2, waiting for transfers between devices, copy_for_each(): return lax.all_to_all(copies, axis, split_axis=0, concat_axis=0, tiled=True)  218 us
    all_to_all x1, blocking collectives, summed_on_arrival(): blocks = lax.all_to_all(in_blocks(shard, dim, size), axis, 0, 0, tiled=True)  119 us
    all_to_all x1, waiting for transfers between devices, summed_on_arrival(): blocks = lax.all_to_all(in_blocks(shard, dim, size), axis, 0, 0, tiled=True)  84.8 us
    transpose x6, local copies, waits for them, and re-layouts, restore_rows(): return jnp.transpose(shaped, (0, 2, 1, 3, 4)).reshape(row_total, col_total)  16.6 us
    all_to_all x1, blocking collectives, relayout(): lax.all_to_all(lax.all_to_all(matrices[5], 'tp', split_axis=0, concat_axi...  16.3 us
    reshape x6, local copies, waits for them, and re-layouts, restore_rows(): return jnp.transpose(shaped, (0, 2, 1, 3, 4)).reshape(row_total, col_total)  15.1 us
  transfers between devices with their start and end apart: 15, of which 15 were waited for; matrix products, arithmetic and copies ran while one was open for 6% of the time, Pallas kernels for 0%

commit v1 on v0

v1 whole, which is shorter than its diff:
```python
import jax
import jax.numpy as jnp
from jax import lax
from jax.sharding import PartitionSpec as P

D = 2048
FF = 5632

norm_eps = 1e-06


def half_step(tokens_t, w_gate, w_up, w_down):
    whole = lax.all_gather(tokens_t, "fs", axis=0, tiled=True)
    widened = whole.astype(jnp.float32)
    row_scale = lax.rsqrt(jnp.sum(widened * widened, axis=0, keepdims=True) / D + norm_eps) * D ** (-0.5)
    g = jnp.dot(w_gate, whole, preferred_element_type=jnp.float32) * row_scale
    u = jnp.dot(w_up, whole, preferred_element_type=jnp.float32) * row_scale
    hidden = (jax.nn.silu(g) * u).astype(jnp.bfloat16)
    partial_value = lax.dot_general(w_down, hidden, (((0,), (0,)), ((), ())), preferred_element_type=jnp.float32)
    summed = lax.psum_scatter(partial_value.astype(jnp.bfloat16), "fs", scatter_dimension=0, tiled=True)
    return (tokens_t.astype(jnp.float32) + 0.5 * FF ** (-0.5) * summed.astype(jnp.float32)).astype(jnp.bfloat16)


def relayout(matrices):
    m = jnp.stack(matrices)
    m = m.reshape(6, 8, 4, 704).transpose(1, 0, 2, 3)
    m = lax.all_to_all(m, "tp", 0, 0, tiled=True)
    m = m.reshape(8, 6, 4, 4, 176).transpose(0, 3, 1, 2, 4).reshape(32, 24, 176)
    m = lax.all_to_all(m, "fs", 0, 0, tiled=True)
    m = lax.all_gather(m.reshape(32 * 24, 176), ("gr", "tp"), axis=0, tiled=True)
    m = m.reshape(2, 8, 32, 6, 4, 176).transpose(3, 5, 0, 2, 1, 4).reshape(6, 176, 2048)
    return tuple(m[i] for i in range(6))


def local(prompt, gain_pre, gate_pre, up_pre, down_pre, gain_post, gate_post, up_post, down_post):
    rounded = (
        (gain_pre[:, None] * gate_pre).astype(jnp.bfloat16),
        (gain_pre[:, None] * up_pre).astype(jnp.bfloat16),
        down_pre.astype(jnp.bfloat16),
        (gain_post[:, None] * gate_post).astype(jnp.bfloat16),
        (gain_post[:, None] * up_post).astype(jnp.bfloat16),
        down_post.astype(jnp.bfloat16),
    )
    served = relayout(rounded)
    middle = half_step(prompt.T, served[0], served[1], served[2])
    result = half_step(middle, served[3], served[4], served[5])
    return (result.T, *served)


def solution(mesh):
    rows = P(("gr", "fs"))
    block = P(("gr", "fs"), "tp")
    tokens = P(("gr", "tp"), "fs")
    return jax.shard_map(
        local,
        mesh=mesh,
        in_specs=(tokens, rows, block, block, block, rows, block, block, block),
        out_specs=(tokens,) + (P("fs", None),) * 6,
        check_vma=False,
    )
```

time: 713 us -> 1140 us (1.60)
  waiting for transfers between devices: 380 us -> 1000 us
  blocking collectives: 135 us -> 51.3 us
  starting transfers between devices: 80.9 us -> 0.38 us
  local copies, waits for them, and re-layouts: 82.1 us -> 50 us
    all_gather x1 -> x3, waiting for transfers between devices: 3.09 us -> 525 us  [the longest x2 379 us: half_step(): whole = lax.all_gather(tokens_t, 'fs', axis=0, tiled=True)]
    reduce_scatter x0 -> x2, waiting for transfers between devices: none -> 475 us  [half_step(): lax.psum_scatter(partial_value.astype(jnp.bfloat16), 'fs', scatter_dimens...]
    all_to_all x14 -> x0, waiting for transfers between devices: 377 us -> none  [the longest x2 218 us: copy_for_each(): return lax.all_to_all(copies, axis, split_axis=0, concat_axis=0, tiled=True)]
    all_to_all x2, blocking collectives: 135 us -> 51.3 us  [the longest x1 37.3 us: relayout(): m = lax.all_to_all(m, 'fs', 0, 0, tiled=True)]
    all_to_all x14 -> x0, starting transfers between devices: 80.7 us -> none  [the longest x1 11.2 us: relayout(): lax.all_to_all(lax.all_to_all(matrices[0], 'tp', split_axis=0, concat_axi...]
    slice x0 -> x7, local copies, waits for them, and re-layouts: none -> 17.8 us  [relayout(): return tuple((m[i] for i in range(6)))]
    reshape x12 -> x4, local copies, waits for them, and re-layouts: 27.3 us -> 10.7 us  [the longest x1 9.93 us: relayout(): m.reshape(2, 8, 32, 6, 4, 176).transpose(3, 5, 0, 2, 1, 4)]
    transpose x6 -> x0, local copies, waits for them, and re-layouts: 16.6 us -> none  [restore_rows(): return jnp.transpose(shaped, (0, 2, 1, 3, 4)).reshape(row_total, col_total)]
  transfers between devices with their start and end apart: 15 -> 5, of which waited for: 15 -> 5; matrix products, arithmetic and copies ran while one was open for 6% -> 2% of each run, Pallas kernels for 0% -> 0%
where the time goes in v1:
time: 1140 us
  waiting for transfers between devices  1000 us (88%)
  blocking collectives  51.3 us (4%)
  local copies, waits for them, and re-layouts  50 us (4%)
  between operations  14 us (1%)
  matrix products  12.1 us (1%)
    reduce_scatter x2, waiting for transfers between devices, half_step(): lax.psum_scatter(partial_value.astype(jnp.bfloat16), 'fs', scatter_dimens...  475 us
    all_gather x2, waiting for transfers between devices, half_step(): whole = lax.all_gather(tokens_t, 'fs', axis=0, tiled=True)  379 us
    all_gather x1, waiting for transfers between devices, relayout(): lax.all_gather(m.reshape(32 * 24, 176), ('gr', 'tp'), axis=0, tiled=True)  146 us
    all_to_all x1, blocking collectives, relayout(): m = lax.all_to_all(m, 'fs', 0, 0, tiled=True)  37.3 us
  transfers between devices with their start and end apart: 5, of which 5 were waited for; matrix products, arithmetic and copies ran while one was open for 2% of the time, Pallas kernels for 0%

profile of v1, /device:TPU:6, one launch (start us, length us, event | category | flops | bytes accessed | tf_op | source)
XLA Modules:
  0.0 1139.1 jit_solution(12735316528702089241)
XLA Ops:
  12.2 14.0 %all_to_all.10 = bf16[8,6,4,704]{3,2,1,0:T(4,128)(2,1)S(1)} all-to-all(bf16[8,6,4,704]{3,2,1,0:T(4,128)(2,1)S(1)} %bitcast.39), channel_id=1, replica_groups=mesh['gr'=2,'fs'=32,'tp'=8] {'tp'}, dimensions={0} | all-to-all | bytes 540672 | tf_op jit(solution)/shard_map/all_to_all | solution.py:27
  27.0 37.3 %all_to_all.11 = bf16[32,24,176]{2,1,0:T(8,128)(2,1)} all-to-all(bf16[32,24,176]{2,1,0:T(8,128)(2,1)S(1)} %copy.61), channel_id=1, replica_groups=mesh['gr'=2,'fs'=32,'tp'=8] {'fs'}, dimensions={0} | all-to-all | bytes 540672 | tf_op jit(solution)/shard_map/all_to_all | solution.py:29
  64.4 173.9 %all-gather.6.cloned.1.call-done = bf16[2048,512]{1,0:T(8,128)(2,1)} async-done(((bf16[64,512]{1,0:T(8,128)(2,1)}), bf16[2048,512]{1,0:T(8,128)(2,1)}) %all-gather.6.cloned.1.call-update) | async-done | bytes 2097168 | tf_op jit(solution)/shard_map/all_gather | solution.py:13
  238.2 2.1 multiply_reduce_fusion.1
  240.3 145.5 %all-gather.4.cloned.1.call-done = bf16[12288,176]{1,0:T(8,128)(2,1)} async-done(((bf16[768,176]{1,0:T(8,128)(2,1)}), bf16[12288,176]{1,0:T(8,128)(2,1)}) %all-gather.4.cloned.1.call-update) | async-done | bytes 4325392 | tf_op jit(solution)/shard_map/all_gather | solution.py:30
  385.9 9.9 reshape.77
  395.8 6.0 fusion.21
  401.8 1.6 copy.50
  403.4 2.5 squeeze.19
  405.9 2.8 copy.49
  408.7 2.5 squeeze.18
  411.2 2.8 copy.51
  414.0 2.5 squeeze.20
  416.4 2.5 convolution_multiply_fusion.3
  418.9 4.8 convolution_convert_fusion.1
  423.8 240.2 %reduce-scatter.3.cloned.1.call-done = bf16[64,512]{1,0:T(8,128)(2,1)} async-done(((bf16[2048,512]{1,0:T(8,128)(2,1)}), bf16[64,512]{1,0:T(8,128)(2,1)}) %reduce-scatter.3.cloned.1.call-update) | async-done | bytes 65552 | tf_op jit(solution)/shard_map/reduce_scatter | solution.py:20
  664.0 1.5 add_convert_fusion.1
  665.8 1.6 copy.53
  667.3 1.7 squeeze.22
  669.0 1.6 copy.52
  670.6 1.7 squeeze.21
  672.3 1.6 copy.54
  673.9 1.7 squeeze.23
  675.6 205.6 %all-gather.8.cloned.1.call-done = bf16[2048,512]{1,0:T(8,128)(2,1)} async-done(((bf16[64,512]{1,0:T(8,128)(2,1)}), bf16[2048,512]{1,0:T(8,128)(2,1)}) %all-gather.8.cloned.1.call-update) | async-done | bytes 2097168 | tf_op jit(solution)/shard_map/all_gather | solution.py:13
  881.2 2.2 multiply_reduce_fusion
  884.1 4.2 convolution_convert_fusion
  890.7 1.2 copy.56
  891.9 1.2 copy.57
  893.1 1.2 copy.58
  894.3 1.2 copy.59
  896.8 234.4 %reduce-scatter.5.cloned.1.call-done = bf16[64,512]{1,0:T(8,128)(2,1)} async-done(((bf16[2048,512]{1,0:T(8,128)(2,1)}), bf16[64,512]{1,0:T(8,128)(2,1)}) %reduce-scatter.5.cloned.1.call-update) | async-done | bytes 65552 | tf_op jit(solution)/shard_map/reduce_scatter | solution.py:20
  1131.1 1.5 fusion.18
  (59 shorter events, 10.4 us)
Async XLA Ops:
  7.2 231.1 %all-gather.6.cloned.1.call-start = ((), (), s32[]{:S(2)}) async-start(), calls=%async_computation.5 | async-start | bytes 2162688 | tf_op jit(solution)/shard_map/all_gather | solution.py:13
  7.9 378.0 %all-gather.4.cloned.1.call-start = ((), (), s32[]{:S(2)}) async-start(), calls=%async_computation.4 | async-start | bytes 6684672 | tf_op jit(solution)/shard_map/all_gather | solution.py:30
  64.3 599.7 %reduce-scatter.3.cloned.1.call-start = ((), (), s32[]{:S(2)}) async-start(), calls=%async_computation.6 | async-start | bytes 2162688 | tf_op jit(solution)/shard_map/reduce_scatter | solution.py:20
  423.8 240.2 %copy-start.11 = (bf16[512,64]{0,1:T(8,128)(2,1)S(1)}, bf16[512,64]{0,1:T(8,128)(2,1)}, u32[]{:S(2)}) copy-start(bf16[512,64]{0,1:T(8,128)(2,1)} %param.9) | copy-start | bytes 196612
  423.8 457.4 %all-gather.8.cloned.1.call-start = ((), (), s32[]{:S(2)}) async-start(), calls=%async_computation.7 | async-start | bytes 2162688 | tf_op jit(solution)/shard_map/all_gather | solution.py:13
  665.5 465.6 %reduce-scatter.5.cloned.1.call-start = ((), (), s32[]{:S(2)}) async-start(), calls=%async_computation.8 | async-start | bytes 2162688 | tf_op jit(solution)/shard_map/reduce_scatter | solution.py:20
  669.0 214.5 %copy-start.3 = (bf16[176,2048]{0,1:T(8,128)(2,1)}, bf16[176,2048]{0,1:T(8,128)(2,1)S(1)}, u32[]{:S(2)}) copy-start(bf16[176,2048]{0,1:T(8,128)(2,1)S(1)} %squeeze.22) | copy-start | bytes 2162692
  672.3 211.8 %copy-start.5 = (bf16[176,2048]{0,1:T(8,128)(2,1)}, bf16[176,2048]{0,1:T(8,128)(2,1)S(1)}, u32[]{:S(2)}) copy-start(bf16[176,2048]{0,1:T(8,128)(2,1)S(1)} %squeeze.21) | copy-start | bytes 2162692
  675.6 208.5 %copy-start.7 = (bf16[176,2048]{0,1:T(8,128)(2,1)}, bf16[176,2048]{0,1:T(8,128)(2,1)S(1)}, u32[]{:S(2)}) copy-start(bf16[176,2048]{0,1:T(8,128)(2,1)S(1)} %squeeze.23) | copy-start | bytes 2162692
  881.2 2.3 copy-start.9
  888.3 1.2 copy-start
  888.3 2.4 copy-start.2
  889.5 2.4 copy-start.1
  890.7 2.4 copy-start.4
  891.9 2.4 copy-start.8
  893.1 2.4 copy-start.6
  894.3 236.8 %copy-start.10 = (bf16[64,512]{1,0:T(8,128)(2,1)S(1)}, bf16[64,512]{1,0:T(8,128)(2,1)}, u32[]{:S(2)}) copy-start(bf16[64,512]{1,0:T(8,128)(2,1)} %add_convert_fusion.1) | copy-start | bytes 196612
Sparse Core Ops, SparseCore 0:
  10.1 228.1 all-gather.5
  241.6 144.2 all-gather.3
  423.9 240.0 reduce-scatter.2
  666.5 214.6 all-gather.7
  888.4 242.6 reduce-scatter.4

commit v2 on v1

v2 whole, which is shorter than its diff:
```python
import jax
import jax.numpy as jnp
from jax import lax
from jax.experimental import pallas as pl
from jax.experimental.pallas import tpu as pltpu
from jax.sharding import PartitionSpec as P

D = 2048
FF = 5632
NX, NY, NZ, NG = 4, 4, 8, 2
WIDTH = 176
FEAT = 64
TOK = 512
PART = 144
HALF = NX * PART
NGRP = 4
GCOL = D // NGRP

norm_eps = 1e-06
MESH = pl.DeviceIdType.MESH


def kernel(*refs):
    (x_ref, wp_ref, res_ref, *outs) = refs[:9]
    (xa, xb, pa, pb, ra, rb, r1, tt, r2, wh) = refs[9:19]
    (ag_s, ag_r, rs_s, rs_r, w1_s, w1_r, w2_s, w2_r, w3_s, w3_r, w4_s, w4_r, w5_s, w5_r, out_s) = refs[19:]

    gr, fs, tp = lax.axis_index("gr"), lax.axis_index("fs"), lax.axis_index("tp")
    y, z = lax.rem(fs, NY), fs // NY
    core, x = lax.rem(tp, 2), tp // 2
    zz = gr * NZ + z

    def wrap(v, n):
        return lax.rem(v + n, n)

    def to_y(v):
        return {"fs": z * NY + v}

    def to_z(v):
        return {"fs": v * NY + y}

    def to_zz(v):
        return {"gr": v // NZ, "fs": lax.rem(v, NZ) * NY + y}

    def to_x(v):
        return {"tp": v * 2 + core}

    sibling = {"tp": x * 2 + 1 - core}
    y_up, y_down, y_far = wrap(y + 1, NY), wrap(y - 1, NY), wrap(y + 2, NY)
    x_up, x_down, x_far = wrap(x + 1, NX), wrap(x - 1, NX), wrap(x + 2, NX)

    def remote(src, dst, s, r, to):
        return pltpu.make_async_remote_copy(src, dst, s, r, device_id=to, device_id_type=MESH)

    barrier = pltpu.get_barrier_semaphore()

    def greet_z(i, _):
        pl.semaphore_signal(barrier, inc=1, device_id=to_zz(lax.rem(zz + i, NG * NZ)), device_id_type=MESH)
        return 0

    lax.fori_loop(1, NG * NZ, greet_z, 0)
    for d in range(1, 4):
        pl.semaphore_signal(barrier, inc=1, device_id=to_y(wrap(y + d, NY)), device_id_type=MESH)
        pl.semaphore_signal(barrier, inc=1, device_id=to_x(wrap(x + d, NX)), device_id_type=MESH)
    pl.semaphore_signal(barrier, inc=1, device_id=sibling, device_id_type=MESH)
    pl.semaphore_wait(barrier, NG * NZ - 1 + 3 + 3 + 1)

    ZP, ZM, YP, YM, YF = range(5)

    def gather_copy(k, buf, kind, zs):
        s, r = ag_s.at[k, kind, zs], ag_r.at[k, kind, zs]
        if kind == ZP:
            blk, to = buf.at[zs, y], to_z(jnp.minimum(z + 1, NZ - 1))
        elif kind == ZM:
            blk, to = buf.at[zs, y], to_z(jnp.maximum(z - 1, 0))
        elif kind == YP:
            blk, to = buf.at[zs, y], to_y(y_up)
        else:
            blk, to = buf.at[zs, y], to_y(y_down)
        return remote(blk, blk, s, r, to)

    def relay_up(k, buf, zs):
        blk = buf.at[zs, y_down]
        return remote(blk, blk, ag_s.at[k, YF, zs], ag_r.at[k, YF, zs], to_y(y_up))

    def relay_down(k, buf, zs):
        blk = buf.at[zs, y_up]
        return remote(blk, blk, ag_s.at[k, YF, zs], ag_r.at[k, YF, zs], to_y(y_down))

    def arrived(k, buf, kind, zs, ys):
        blk = buf.at[zs, ys]
        remote(blk, blk, ag_s.at[k, kind, zs], ag_r.at[k, kind, zs], to_y(y_up)).wait_recv()

    def gather_along_z(k, buf, t):
        lower, upper = z - t, z + t

        @pl.when(lower >= 0)
        def _():
            @pl.when(t > 0)
            def _():
                arrived(k, buf, ZP, lower, y)

            @pl.when(z < NZ - 1)
            def _():
                gather_copy(k, buf, ZP, lower).start()

            gather_copy(k, buf, YP, lower).start()
            gather_copy(k, buf, YM, lower).start()

        @pl.when(upper < NZ)
        def _():
            @pl.when(t > 0)
            def _():
                arrived(k, buf, ZM, upper, y)

            @pl.when(z > 0)
            def _():
                gather_copy(k, buf, ZM, upper).start()

            @pl.when(t > 0)
            def _():
                gather_copy(k, buf, YP, upper).start()
                gather_copy(k, buf, YM, upper).start()

    def gather_relay_one(k, buf, zs):
        arrived(k, buf, YP, zs, y_down)

        @pl.when(lax.rem(zs, 2) == 0)
        def _():
            relay_up(k, buf, zs).start()

        arrived(k, buf, YM, zs, y_up)

        @pl.when(lax.rem(zs, 2) == 1)
        def _():
            relay_down(k, buf, zs).start()

    def gather_relay(k, buf, t):
        @pl.when((t >= 0) & (z - t >= 0))
        def _():
            gather_relay_one(k, buf, z - t)

        @pl.when((t > 0) & (z + t < NZ))
        def _():
            gather_relay_one(k, buf, z + t)

    LAG = 2

    def gather_rounds(k, buf, first, last):
        def step(t, _):
            @pl.when(t < NZ)
            def _():
                gather_along_z(k, buf, t)

            gather_relay(k, buf, t - LAG)
            return 0

        lax.fori_loop(first, last, step, 0)

    def gather_end(k, buf):
        def step(zs, _):
            arrived(k, buf, YF, zs, y_far)
            return 0

        lax.fori_loop(0, NZ, step, 0)

    def gather_drain(k, buf):
        def step(zs, _):
            @pl.when((zs <= z) & (z < NZ - 1))
            def _():
                gather_copy(k, buf, ZP, zs).wait_send()

            @pl.when((zs >= z) & (z > 0))
            def _():
                gather_copy(k, buf, ZM, zs).wait_send()

            gather_copy(k, buf, YP, zs).wait_send()
            gather_copy(k, buf, YM, zs).wait_send()
            relay_up(k, buf, zs).wait_send()
            return 0

        lax.fori_loop(0, NZ, step, 0)

    FB, UP, DN = 4, 2, 3

    def send_part(k, part, land, kind, zd, col, to):
        return remote(part.at[zd, col], land.at[kind, zd], rs_s.at[k, kind, zd], rs_r.at[k, kind, zd], to)

    def landed(k, part, land, kind, zd):
        send_part(k, part, land, kind, zd, y, to_y(y_up)).wait_recv()

    def sum_far(k, part, land, zd):
        @pl.when(lax.rem(zd, 2) == 0)
        def _():
            send_part(k, part, land, FB, zd, y_far, to_y(y_up)).start()

        @pl.when(lax.rem(zd, 2) == 1)
        def _():
            send_part(k, part, land, FB, zd, y_far, to_y(y_down)).start()

    def sum_near(k, part, land, zd):
        landed(k, part, land, FB, zd)
        target = jnp.where(lax.rem(zd, 2) == 0, y_up, y_down)
        part[zd, target] = (part[zd, target].astype(jnp.float32) + land[FB, zd].astype(jnp.float32)).astype(jnp.bfloat16)
        send_part(k, part, land, UP, zd, y_up, to_y(y_up)).start()
        send_part(k, part, land, DN, zd, y_down, to_y(y_down)).start()

    def column_sum(k, part, land, zd):
        landed(k, part, land, UP, zd)
        landed(k, part, land, DN, zd)
        return part[zd, y].astype(jnp.float32) + land[UP, zd].astype(jnp.float32) + land[DN, zd].astype(jnp.float32)

    def sum_upward(k, part, land, zd):
        part[zd, y] = column_sum(k, part, land, zd).astype(jnp.bfloat16)

        @pl.when(z > 0)
        def _():
            landed(k, part, land, ZP, zd)
            part[zd, y] = (part[zd, y].astype(jnp.float32) + land[ZP, zd].astype(jnp.float32)).astype(jnp.bfloat16)

        send_part(k, part, land, ZP, zd, y, to_z(jnp.minimum(z + 1, NZ - 1))).start()

    def sum_downward(k, part, land, zd):
        part[zd, y] = column_sum(k, part, land, zd).astype(jnp.bfloat16)

        @pl.when(z < NZ - 1)
        def _():
            landed(k, part, land, ZM, zd)
            part[zd, y] = (part[zd, y].astype(jnp.float32) + land[ZM, zd].astype(jnp.float32)).astype(jnp.bfloat16)

        send_part(k, part, land, ZM, zd, y, to_z(jnp.maximum(z - 1, 0))).start()

    def at_distance(t, f_up, f_down):
        @pl.when((t > 0) & (t < NZ) & (z + t < NZ))
        def _():
            f_up(z + t)

        @pl.when((t >= 0) & (t < NZ) & (z - t >= 0))
        def _():
            f_down(z - t)

    def sum_rounds(k, part, land):
        def step(s, _):
            t = NZ - 1 - s
            at_distance(t, lambda zd: sum_far(k, part, land, zd), lambda zd: sum_far(k, part, land, zd))
            at_distance(t + 1, lambda zd: sum_near(k, part, land, zd), lambda zd: sum_near(k, part, land, zd))
            at_distance(
                jnp.where(t + 2 > 0, t + 2, NZ),
                lambda zd: sum_upward(k, part, land, zd),
                lambda zd: sum_downward(k, part, land, zd),
            )
            return 0

        lax.fori_loop(0, NZ + 1, step, 0)
        total = column_sum(k, part, land, z)
        part[z, y] = total.astype(jnp.bfloat16)

    def sum_result(k, part, land, own):
        sum_rounds(k, part, land)

        @pl.when(z > 0)
        def _():
            landed(k, part, land, ZP, z)

        @pl.when(z < NZ - 1)
        def _():
            landed(k, part, land, ZM, z)

        low = jnp.where(z > 0, land[ZP, z].astype(jnp.float32), 0.0)
        high = jnp.where(z < NZ - 1, land[ZM, z].astype(jnp.float32), 0.0)
        total = part[z, y].astype(jnp.float32) + low + high
        return (own.astype(jnp.float32) + 0.5 * FF ** (-0.5) * total).astype(jnp.bfloat16)

    def sum_drain(k, part, land):
        def step(zd, _):
            for kind in (FB, UP, DN):
                send_part(k, part, land, kind, zd, y, to_y(y_up)).wait_send()

            @pl.when(zd > z)
            def _():
                send_part(k, part, land, ZP, zd, y, to_y(y_up)).wait_send()

            @pl.when(zd < z)
            def _():
                send_part(k, part, land, ZM, zd, y, to_y(y_up)).wait_send()

            return 0

        lax.fori_loop(0, NZ, step, 0)

    def w1_copy(d):
        return remote(
            wp_ref.at[wrap(y + d, NY)], r1.at[pl.ds(y * 32, 32)], w1_s.at[d - 1], w1_r.at[d - 1], to_y(wrap(y + d, NY))
        )

    def w2_copy(h, d):
        xd = wrap(x + d, NX)
        return remote(
            tt.at[pl.ds(pl.multiple_of(h * HALF + xd * PART, 16), PART)],
            r2.at[h, x],
            w2_s.at[h, d - 1],
            w2_r.at[h, d - 1],
            to_x(xd),
        )

    def my_rows(p):
        return pl.ds(pl.multiple_of(p * PART, 16), PART)

    def w3_target(i):
        return lax.rem(i, 2) * NZ + (i // 2) * 2 + core

    def w3_block(h):
        return wh.at[h, my_rows(x), pl.ds(pl.multiple_of(zz * 128, 128), 128)]

    def w3_copy(h, i):
        return remote(r2.at[h, i // 2], w3_block(h), w3_s.at[h, i], w3_r.at[h, zz], to_zz(w3_target(i)))

    def w3_local(h, i):
        return pltpu.make_async_copy(r2.at[h, i // 2], w3_block(h), w3_s.at[h, i])

    def w3_start(h):
        def step(i, _):
            @pl.when(w3_target(i) == zz)
            def _():
                w3_local(h, i).start()

            @pl.when(w3_target(i) != zz)
            def _():
                w3_copy(h, i).start()

            return 0

        lax.fori_loop(0, 2 * NX, step, 0)

    def w3_done(h):
        def step(i, _):
            @pl.when(w3_target(i) == zz)
            def _():
                w3_local(h, i).wait()

            @pl.when(w3_target(i) != zz)
            def _():
                w3_copy(h, i).wait_send()

            return 0

        lax.fori_loop(0, 2 * NX, step, 0)

    def w3_arrive(h, g):
        def step(i, _):
            @pl.when(i != zz)
            def _():
                remote(
                    r2.at[h, 0],
                    wh.at[h, my_rows(x), pl.ds(pl.multiple_of(i * 128, 128), 128)],
                    w3_s.at[h, 0],
                    w3_r.at[h, i],
                    sibling,
                ).wait_recv()

            return 0

        per = NG * NZ // NGRP
        lax.fori_loop(g * per, (g + 1) * per, step, 0)

    def w4_copy(h, kind, p, g, to):
        blk = wh.at[h, my_rows(p), pl.ds(g * GCOL, GCOL)]
        return remote(blk, blk, w4_s.at[h, kind, g], w4_r.at[h, kind, g], to)

    def w5_copy(h, kind, p):
        blk = wh.at[h, my_rows(p)]
        return remote(blk, blk, w5_s.at[h, kind], w5_r.at[h, kind], sibling)

    hub = core == lax.rem(z, 2)

    def w4_send(h):
        w3_done(h)

        @pl.when(hub)
        def _():
            for g in range(NGRP):
                w3_arrive(h, g)
                w4_copy(h, 0, x, g, to_x(x_up)).start()
                w4_copy(h, 1, x, g, to_x(x_down)).start()
            w5_copy(h, 0, x).start()

    def w4_relay(h):
        @pl.when(hub)
        def _():
            for g in range(NGRP):
                w4_copy(h, 0, x_down, g, to_x(x_up)).wait_recv()
                if g % 2 == 0:
                    w4_copy(h, 2, x_down, g, to_x(x_up)).start()
                w4_copy(h, 1, x_up, g, to_x(x_down)).wait_recv()
                if g % 2 == 1:
                    w4_copy(h, 2, x_up, g, to_x(x_down)).start()
            w5_copy(h, 1, x_down).start()
            w5_copy(h, 2, x_up).start()

    def w5_end(h):
        @pl.when(hub)
        def _():
            for g in range(NGRP):
                w4_copy(h, 2, x_far, g, to_x(x_up)).wait_recv()
            w5_copy(h, 3, x_far).start()

        @pl.when(jnp.logical_not(hub))
        def _():
            for kind, p in enumerate((x, x_down, x_up, x_far)):
                w5_copy(h, kind, p).wait_recv()

    def w_drain(h):
        @pl.when(hub)
        def _():
            for kind, p in enumerate((x, x_down, x_up, x_far)):
                w5_copy(h, kind, p).wait_send()
            for kind in range(3):
                for g in range(NGRP):
                    w4_copy(h, kind, x, g, to_x(x_up)).wait_send()

    def out_copy(h, m):
        return pltpu.make_async_copy(wh.at[h, pl.ds(m * WIDTH, WIDTH)], outs[h * 3 + m], out_s.at[h * 3 + m])

    def products(h, buf, part):
        whole = buf[...].reshape(D, TOK)
        wide = whole.astype(jnp.float32)
        squares = jnp.sum(wide * wide, axis=0, keepdims=True)
        row_scale = lax.rsqrt(squares / D + norm_eps) * D ** (-0.5)
        both = jnp.dot(wh[h, 0 : 2 * WIDTH], whole, preferred_element_type=jnp.float32)
        g = both[:WIDTH] * row_scale
        u = both[WIDTH:] * row_scale
        hidden = (g / (1.0 + jnp.exp(-g)) * u).astype(jnp.bfloat16)

        def step(zd, _):
            w = wh[h, 2 * WIDTH : 3 * WIDTH, pl.ds(pl.multiple_of(zd * 256, 256), 256)]
            p = lax.dot_general(w, hidden, (((0,), (0,)), ((), ())), preferred_element_type=jnp.float32)
            part[zd] = p.astype(jnp.bfloat16).reshape(NY, FEAT, TOK)
            return 0

        lax.fori_loop(0, NZ, step, 0)

    for d in range(1, 4):
        w1_copy(d).start()
    xa[z, y] = x_ref[...]
    r1[pl.ds(y * 32, 32), :] = wp_ref[y]
    gather_rounds(0, xa, 0, 1)
    for d in range(1, 4):
        remote(
            wp_ref.at[0], r1.at[pl.ds(wrap(y - d, NY) * 32, 32)], w1_s.at[d - 1], w1_r.at[d - 1], to_y(y_up)
        ).wait_recv()
    for k in range(9):
        tt[k * 128 : (k + 1) * 128, :] = r1[:, k * 128 : (k + 1) * 128].astype(jnp.float32).T.astype(jnp.bfloat16)
    for h in range(2):
        for d in range(1, 4):
            w2_copy(h, d).start()
        r2[h, x] = tt[pl.ds(pl.multiple_of(h * HALF + x * PART, 16), PART), :]

    def w2_wait(h):
        for d in range(1, 4):
            remote(r2.at[h, 0], r2.at[h, wrap(x - d, NX)], w2_s.at[h, d - 1], w2_r.at[h, d - 1], to_x(x_up)).wait_recv()

    gather_rounds(0, xa, 1, 3)
    w2_wait(0)
    w3_start(0)
    gather_rounds(0, xa, 3, NZ + LAG)
    w4_send(0)
    gather_end(0, xa)
    w4_relay(0)
    w5_end(0)
    products(0, xa, pa)
    w2_wait(1)
    w3_start(1)
    for m in range(3):
        out_copy(0, m).start()
    xb[z, y] = sum_result(0, pa, ra, x_ref[...])
    w4_send(1)
    gather_rounds(1, xb, 0, 2)
    w4_relay(1)
    gather_rounds(1, xb, 2, NZ + LAG)
    gather_end(1, xb)
    w5_end(1)
    for m in range(3):
        out_copy(1, m).start()
    products(1, xb, pb)
    res_ref[...] = sum_result(1, pb, rb, xb[z, y])

    for d in range(1, 4):
        w1_copy(d).wait_send()
        for h in range(2):
            w2_copy(h, d).wait_send()
    for h in range(2):
        w_drain(h)
    gather_drain(0, xa)
    gather_drain(1, xb)
    sum_drain(0, pa, ra)
    sum_drain(1, pb, rb)
    for h in range(2):
        for m in range(3):
            out_copy(h, m).wait()


def packed(gate, up, down):
    three = jnp.stack([m.reshape(32, NY, WIDTH) for m in (gate, up, down)], axis=2)
    return jnp.pad(three.reshape(32, NY, 3 * WIDTH), ((0, 0), (0, 0), (0, HALF - 3 * WIDTH)))


def local(prompt, gain_pre, gate_pre, up_pre, down_pre, gain_post, gate_post, up_post, down_post):
    first = packed(
        (gain_pre[:, None] * gate_pre).astype(jnp.bfloat16),
        (gain_pre[:, None] * up_pre).astype(jnp.bfloat16),
        down_pre.astype(jnp.bfloat16),
    )
    second = packed(
        (gain_post[:, None] * gate_post).astype(jnp.bfloat16),
        (gain_post[:, None] * up_post).astype(jnp.bfloat16),
        down_post.astype(jnp.bfloat16),
    )
    wp = jnp.transpose(jnp.concatenate([first, second], axis=2), (1, 0, 2))
    block = jax.ShapeDtypeStruct((WIDTH, D), jnp.bfloat16)
    vm = pl.BlockSpec(memory_space=pltpu.VMEM)
    dma = pltpu.SemaphoreType.DMA
    bf = jnp.bfloat16
    res, *served = pl.pallas_call(
        kernel,
        out_shape=(jax.ShapeDtypeStruct((FEAT, TOK), bf),) + (block,) * 6,
        in_specs=[vm, vm],
        out_specs=(vm,) + (pl.BlockSpec(memory_space=pl.ANY),) * 6,
        scratch_shapes=[
            pltpu.VMEM((NZ, NY, FEAT, TOK), bf),
            pltpu.VMEM((NZ, NY, FEAT, TOK), bf),
            pltpu.VMEM((NZ, NY, FEAT, TOK), bf),
            pltpu.VMEM((NZ, NY, FEAT, TOK), bf),
            pltpu.VMEM((5, NZ, FEAT, TOK), bf),
            pltpu.VMEM((5, NZ, FEAT, TOK), bf),
            pltpu.VMEM((128, 2 * HALF), bf),
            pltpu.VMEM((2 * HALF, 128), bf),
            pltpu.VMEM((2, NX, PART, 128), bf),
            pltpu.VMEM((2, HALF, D), bf),
            dma((2, 5, NZ)),
            dma((2, 5, NZ)),
            dma((2, 5, NZ)),
            dma((2, 5, NZ)),
            dma((3,)),
            dma((3,)),
            dma((2, 3)),
            dma((2, 3)),
            dma((2, 2 * NX)),
            dma((2, NG * NZ)),
            dma((2, 3, NGRP)),
            dma((2, 3, NGRP)),
            dma((2, 4)),
            dma((2, 4)),
            dma((6,)),
        ],
        compiler_params=pltpu.CompilerParams(
            collective_id=0, has_side_effects=True, vmem_limit_bytes=56 * 1024 * 1024
        ),
    )(prompt.T, wp)
    return (res.T, *served)


def solution(mesh):
    rows = P(("gr", "fs"))
    block = P(("gr", "fs"), "tp")
    tokens = P(("gr", "tp"), "fs")
    return jax.shard_map(
        local,
        mesh=mesh,
        in_specs=(tokens, rows, block, block, block, rows, block, block, block),
        out_specs=(tokens,) + (P("fs", None),) * 6,
        check_vma=False,
    )
```

time: 1140 us -> 198 us (0.17)
  waiting for transfers between devices: 1000 us -> 0 us
  Pallas kernels: 0 us -> 178 us
  blocking collectives: 51.3 us -> 0 us
  local copies, waits for them, and re-layouts: 50 us -> 13.1 us
  between operations: 14 us -> 0.86 us
  matrix products: 12.1 us -> 0 us
    all_gather x3 -> x0, waiting for transfers between devices: 525 us -> none  [the longest x2 379 us: half_step(): whole = lax.all_gather(tokens_t, 'fs', axis=0, tiled=True)]
    reduce_scatter x2 -> x0, waiting for transfers between devices: 475 us -> none  [half_step(): lax.psum_scatter(partial_value.astype(jnp.bfloat16), 'fs', scatter_dimens...]
    pallas_call x0 -> x1, Pallas kernels: none -> 178 us  [local(): pl.pallas_call(kernel, out_shape=(jax.ShapeDtypeStruct((FEAT, TOK), bf),)...]
    all_to_all x2 -> x0, blocking collectives: 51.3 us -> none  [the longest x1 37.3 us: relayout(): m = lax.all_to_all(m, 'fs', 0, 0, tiled=True)]
    slice x7 -> x0, local copies, waits for them, and re-layouts: 17.8 us -> none  [relayout(): return tuple((m[i] for i in range(6)))]
    squeeze x6 -> x0, local copies, waits for them, and re-layouts: 12.6 us -> none  [relayout(): return tuple((m[i] for i in range(6)))]
    dot_general x4 -> x0, matrix products: 12.1 us -> none  [the longest x2 9 us: half_step(): lax.dot_general(w_down, hidden, (((0,), (0,)), ((), ())), preferred_eleme...]
  transfers between devices with their start and end apart: 5 -> 0, of which waited for: 5 -> 0; matrix products, arithmetic and copies ran while one was open for 2% -> 0% of each run, Pallas kernels for 0% -> 0%
where the time goes in v2:
time: 198 us; the launch traced here: 195 us
  Pallas kernels  178 us (90%)
  local copies, waits for them, and re-layouts  13.1 us (7%)
  other arithmetic  2.94 us (1%)
    pallas_call x1, Pallas kernels, local(): pl.pallas_call(kernel, out_shape=(jax.ShapeDtypeStruct((FEAT, TOK), bf),)...  178 us
    unnamed x31, local copies, waits for them, and re-layouts  11.5 us

profile of v2, /device:TPU:6, one launch (start us, length us, event | category | flops | bytes accessed | tf_op | source)
XLA Modules:
  0.0 194.9 jit_solution(9498892625623083781)
XLA Ops:
  0.6 0.9 convert_element_type.23
  1.6 0.1 stack_reshape.20
  1.7 0.1 stack_reshape.23
  1.8 0.1 copy.27
  2.0 0.1 copy.24
  2.1 0.4 copy-done.10
  2.5 0.4 copy-done.6
  3.0 0.1 stack_reshape.18
  3.1 0.1 copy.22
  3.2 0.1 stack_reshape.19
  3.3 0.1 copy.23
  3.4 0.5 pad_maximum_fusion
  4.0 0.2 reshape.22
  4.1 0.7 copy-done.8
  5.1 0.1 copy.25
  5.2 0.1 stack_reshape.22
  5.3 0.1 copy.26
  5.4 0.5 pad_maximum_fusion.1
  5.9 0.2 reshape.23
  6.1 0.8 fusion.3.refs_1_
  6.9 178.1 %shard_map.144 = (bf16[64,512]{1,0:T(8,128)(2,1)}, bf16[176,2048]{1,0:T(8,128)(2,1)}, bf16[176,2048]{1,0:T(8,128)(2,1)}, bf16[176,2048]{1,0:T(8,128)(2,1)}, bf16...) custom-call(bf16[64,512]{1,0:T(8,128)(2,1)} %bitcast.9, ...), custom_call_target="tpu_custom_call" | custom-call | tf_op jit(solution)/shard_map/pallas_call | solution.py:523
  185.0 1.5 copy.35
  186.5 2.1 %copy.36 = bf16[176,2048]{1,0:T(8,128)(2,1)} copy(bf16[176,2048]{1,0:T(8,128)(2,1)} %get-tuple-element.33) | data formatting | bytes 1441792
  188.6 0.9 copy.37
  189.5 0.5 copy-done.3
  190.0 0.9 copy.38
  190.8 0.5 copy-done.2
  191.3 0.9 copy.39
  192.2 0.5 copy-done.1
  192.7 0.9 copy.40
  193.6 0.5 copy-done
  194.1 0.9 copy.41
  (21 shorter events, 0.4 us)
Async XLA Ops:
  0.6 1.1 copy-start.5
  1.8 0.7 copy-start.10
  1.9 0.9 copy-start.6
  2.0 0.9 copy-start.7
  3.9 0.9 copy-start.8
  3.9 0.9 copy-start.9
  3.9 0.9 copy-start.11
  186.5 2.1 %copy-start.4 = (bf16[176,2048]{1,0:T(8,128)(2,1)S(1)}, bf16[176,2048]{1,0:T(8,128)(2,1)}, u32[]{:S(2)}) copy-start(bf16[176,2048]{1,0:T(8,128)(2,1)} %get-tuple-element.34) | copy-start | bytes 2162692
  188.6 1.4 copy-start.3
  190.0 1.4 copy-start.2
  191.3 1.4 copy-start.1
  192.7 1.4 copy-start

commit v3 on v1

v3 whole, which is shorter than its diff:
```python
import jax
import jax.numpy as jnp
from jax import lax
from jax.experimental import pallas as pl
from jax.experimental.pallas import tpu as pltpu
from jax.sharding import PartitionSpec as P

D = 2048
FF = 5632
NX, NY, NZ, NG = 4, 4, 8, 2
WIDTH = 176
FEAT = 64
TOK = 512
PART = 48
ROWS = NX * PART
NGRP = 2
GCOL = D // NGRP
EXPRESS = 4

norm_eps = 1e-06
MESH = pl.DeviceIdType.MESH


def kernel(
    x_ref, gain_a, gain_b, *refs
):
    mats, res_ref, outs = refs[:6], refs[6], refs[7:13]
    (xa, xb, pa, pb, ra, rb, wp, r1, tt, r2, wh, gains, loaded) = refs[13:26]
    (ag_s, ag_r, rs_s, rs_r, w1_s, w1_r, w2_s, w2_r, w3_s, w3_r, w4_s, w4_r, w5_s, w5_r, in_s, out_s) = refs[26:]

    gr, fs, tp = lax.axis_index("gr"), lax.axis_index("fs"), lax.axis_index("tp")
    y, z = lax.rem(fs, NY), fs // NY
    core, x = lax.rem(tp, 2), tp // 2
    zz = gr * NZ + z

    loads = [pltpu.make_async_copy(m, loaded.at[i], in_s.at[i]) for i, m in enumerate(mats)]
    loads.append(pltpu.make_async_copy(gain_a, gains.at[0], in_s.at[6]))
    loads.append(pltpu.make_async_copy(gain_b, gains.at[1], in_s.at[7]))
    loads.append(pltpu.make_async_copy(x_ref, xa.at[z, y], in_s.at[8]))
    for c in loads:
        c.start()

    def wrap(v, n):
        return lax.rem(v + n, n)

    def to_y(v):
        return {"fs": z * NY + v}

    def to_z(v):
        return {"fs": v * NY + y}

    def to_zz(v):
        return {"gr": v // NZ, "fs": lax.rem(v, NZ) * NY + y}

    def to_x(v):
        return {"tp": v * 2 + core}

    sibling = {"tp": x * 2 + 1 - core}
    y_up, y_down, y_far = wrap(y + 1, NY), wrap(y - 1, NY), wrap(y + 2, NY)
    x_up, x_down, x_far = wrap(x + 1, NX), wrap(x - 1, NX), wrap(x + 2, NX)

    def remote(src, dst, s, r, to):
        return pltpu.make_async_remote_copy(src, dst, s, r, device_id=to, device_id_type=MESH)

    barrier = pltpu.get_barrier_semaphore()

    def greet_z(i, _):
        pl.semaphore_signal(barrier, inc=1, device_id=to_zz(lax.rem(zz + i, NG * NZ)), device_id_type=MESH)
        return 0

    lax.fori_loop(1, NG * NZ, greet_z, 0)
    for d in range(1, 4):
        pl.semaphore_signal(barrier, inc=1, device_id=to_y(wrap(y + d, NY)), device_id_type=MESH)
        pl.semaphore_signal(barrier, inc=1, device_id=to_x(wrap(x + d, NX)), device_id_type=MESH)
    pl.semaphore_signal(barrier, inc=1, device_id=sibling, device_id_type=MESH)

    def pack(h):
        eye = lax.broadcasted_iota(jnp.int32, (32, 32), 0) == lax.broadcasted_iota(jnp.int32, (32, 32), 1)
        gain = jnp.sum(jnp.where(eye, jnp.broadcast_to(gains[h], (32, 32)), 0.0), axis=1, keepdims=True)
        for m in range(3):
            v = loaded[h * 3 + m]
            v = v * gain if m < 2 else v
            for at in range(NY):
                piece = jnp.pad(v[:, at * WIDTH : (at + 1) * WIDTH], ((0, 0), (0, ROWS - WIDTH)))
                wp[h, at, :, m * ROWS : (m + 1) * ROWS] = piece.astype(jnp.bfloat16)

    for c in loads:
        c.wait()
    pack(0)
    pack(1)
    for h in range(2):
        r1[h, pl.ds(y * 32, 32), :] = wp[h, y]
    pl.semaphore_wait(barrier, NG * NZ - 1 + 3 + 3 + 1)

    STEPS = 6

    def each(s, f_low, f_high):
        d1 = s + jnp.where(s >= 4, 2, 0)
        fits = (s >= 0) & (s < STEPS)

        @pl.when(fits & (z - d1 >= 0))
        def _():
            f_low(z - d1, d1)

        @pl.when(fits & (d1 > 0) & (z + d1 < NZ))
        def _():
            f_high(z + d1, d1)

        d2 = s + 2
        second = (s == 2) | (s == 3)

        @pl.when(second & (z - d2 >= 0))
        def _():
            f_low(z - d2, d2)

        @pl.when(second & (z + d2 < NZ))
        def _():
            f_high(z + d2, d2)

    z_up, z_down = jnp.minimum(z + 1, NZ - 1), jnp.maximum(z - 1, 0)
    z_far_up, z_far_down = jnp.minimum(z + EXPRESS, NZ - 1), jnp.maximum(z - EXPRESS, 0)

    ZP, ZM, UP, DN, FB, XP, XM = range(7)

    def block_copy(k, buf, kind, zs, ys, to, s_kind=None):
        blk = buf.at[zs, ys]
        s_kind = kind if s_kind is None else s_kind
        return remote(blk, blk, ag_s.at[k, s_kind, zs], ag_r.at[k, kind, zs], to)

    def arrived(k, buf, kind, zs, ys):
        block_copy(k, buf, kind, zs, ys, to_y(y_up)).wait_recv()

    def along_y(k, buf, zs):
        block_copy(k, buf, UP, zs, y, to_y(y_up)).start()
        block_copy(k, buf, DN, zs, y, to_y(y_down)).start()

    def gather_low(k, buf, zs, d):
        @pl.when(d > 0)
        def _():
            arrived(k, buf, ZP, zs, y)

        @pl.when((z < NZ - 1) & (d != EXPRESS - 1))
        def _():
            block_copy(k, buf, ZP, zs, y, to_z(z_up)).start()

        @pl.when(d == 0)
        def _():
            @pl.when(z > 0)
            def _():
                block_copy(k, buf, ZM, zs, y, to_z(z_down)).start()

            @pl.when(z + EXPRESS < NZ)
            def _():
                block_copy(k, buf, ZP, zs, y, to_z(z_far_up), XP).start()

            @pl.when(z - EXPRESS >= 0)
            def _():
                block_copy(k, buf, ZM, zs, y, to_z(z_far_down), XM).start()

        along_y(k, buf, zs)

    def gather_high(k, buf, zs, d):
        arrived(k, buf, ZM, zs, y)

        @pl.when((z > 0) & (d != EXPRESS - 1))
        def _():
            block_copy(k, buf, ZM, zs, y, to_z(z_down)).start()

        along_y(k, buf, zs)

    def gather_relay(k, buf, zs):
        arrived(k, buf, UP, zs, y_down)

        @pl.when(lax.rem(zs, 2) == 0)
        def _():
            block_copy(k, buf, FB, zs, y_down, to_y(y_up)).start()

        arrived(k, buf, DN, zs, y_up)

        @pl.when(lax.rem(zs, 2) == 1)
        def _():
            block_copy(k, buf, FB, zs, y_up, to_y(y_down)).start()

    LAG = 2

    def gather_rounds(k, buf, first, last):
        def step(s, _):
            each(s, lambda zs, d: gather_low(k, buf, zs, d), lambda zs, d: gather_high(k, buf, zs, d))
            each(s - LAG, lambda zs, d: gather_relay(k, buf, zs), lambda zs, d: gather_relay(k, buf, zs))
            return 0

        lax.fori_loop(first, last, step, 0)

    def gather_end(k, buf):
        def step(zs, _):
            arrived(k, buf, FB, zs, y_far)
            return 0

        lax.fori_loop(0, NZ, step, 0)

    def gather_drain(k, buf):
        def sent(kind, zs):
            block_copy(k, buf, kind, zs, y, to_y(y_up)).wait_send()

        def step(zs, _):
            @pl.when((zs <= z) & (z < NZ - 1) & (z - zs != EXPRESS - 1))
            def _():
                sent(ZP, zs)

            @pl.when((zs >= z) & (z > 0) & (zs - z != EXPRESS - 1))
            def _():
                sent(ZM, zs)

            sent(UP, zs)
            sent(DN, zs)
            sent(FB, zs)
            return 0

        lax.fori_loop(0, NZ, step, 0)

        @pl.when(z + EXPRESS < NZ)
        def _():
            sent(XP, z)

        @pl.when(z - EXPRESS >= 0)
        def _():
            sent(XM, z)

    def send_part(k, part, land, kind, zd, col, to):
        return remote(part.at[zd, col], land.at[kind, zd], rs_s.at[k, kind, zd], rs_r.at[k, kind, zd], to)

    def landed(k, part, land, kind, zd):
        send_part(k, part, land, kind, zd, y, to_y(y_up)).wait_recv()

    def sum_far(k, part, land, zd):
        @pl.when(lax.rem(zd, 2) == 0)
        def _():
            send_part(k, part, land, FB, zd, y_far, to_y(y_up)).start()

        @pl.when(lax.rem(zd, 2) == 1)
        def _():
            send_part(k, part, land, FB, zd, y_far, to_y(y_down)).start()

    def sum_near(k, part, land, zd):
        landed(k, part, land, FB, zd)
        target = jnp.where(lax.rem(zd, 2) == 0, y_up, y_down)
        part[zd, target] = (part[zd, target].astype(jnp.float32) + land[FB, zd].astype(jnp.float32)).astype(jnp.bfloat16)
        send_part(k, part, land, UP, zd, y_up, to_y(y_up)).start()
        send_part(k, part, land, DN, zd, y_down, to_y(y_down)).start()

    def column_sum(k, part, land, zd):
        landed(k, part, land, UP, zd)
        landed(k, part, land, DN, zd)
        return part[zd, y].astype(jnp.float32) + land[UP, zd].astype(jnp.float32) + land[DN, zd].astype(jnp.float32)

    def sum_along_z(k, part, land, zd, d, chain, express, more, to_next, to_far):
        own = column_sum(k, part, land, zd)

        @pl.when(jnp.logical_not(more & (d != EXPRESS - 1)))
        def _():
            part[zd, y] = own.astype(jnp.bfloat16)

        @pl.when(more & (d != EXPRESS - 1))
        def _():
            landed(k, part, land, chain, zd)
            part[zd, y] = (own + land[chain, zd].astype(jnp.float32)).astype(jnp.bfloat16)

        @pl.when(d != EXPRESS)
        def _():
            send_part(k, part, land, chain, zd, y, to_next).start()

        @pl.when(d == EXPRESS)
        def _():
            send_part(k, part, land, express, zd, y, to_far).start()

    def sum_upward(k, part, land, zd, d):
        sum_along_z(k, part, land, zd, d, ZP, XP, z > 0, to_z(z_up), to_z(z_far_up))

    def sum_downward(k, part, land, zd, d):
        @pl.when(d > 0)
        def _():
            sum_along_z(k, part, land, zd, d, ZM, XM, z < NZ - 1, to_z(z_down), to_z(z_far_down))

    def sum_result(k, part, land, own):
        def step(i, _):
            s = STEPS - 1 - i
            each(s, lambda zd, d: sum_far(k, part, land, zd), lambda zd, d: sum_far(k, part, land, zd))
            each(s + 1, lambda zd, d: sum_near(k, part, land, zd), lambda zd, d: sum_near(k, part, land, zd))
            each(
                s + 2,
                lambda zd, d: sum_downward(k, part, land, zd, d),
                lambda zd, d: sum_upward(k, part, land, zd, d),
            )
            return 0

        lax.fori_loop(0, STEPS + 1, step, 0)
        total = column_sum(k, part, land, z)
        for kind, there in ((ZP, z > 0), (ZM, z < NZ - 1), (XP, z - EXPRESS >= 0), (XM, z + EXPRESS < NZ)):

            @pl.when(there)
            def _(kind=kind):
                landed(k, part, land, kind, z)

            @pl.when(jnp.logical_not(there))
            def _(kind=kind):
                land[kind, z] = jnp.zeros((FEAT, TOK), jnp.bfloat16)

            total = total + land[kind, z].astype(jnp.float32)
        return (own.astype(jnp.float32) + 0.5 * FF ** (-0.5) * total).astype(jnp.bfloat16)

    def sum_drain(k, part, land):
        def sent(kind, zd):
            send_part(k, part, land, kind, zd, y, to_y(y_up)).wait_send()

        def step(zd, _):
            for kind in (FB, UP, DN):
                sent(kind, zd)

            @pl.when((zd > z) & (zd - z != EXPRESS))
            def _():
                sent(ZP, zd)

            @pl.when((zd < z) & (z - zd != EXPRESS))
            def _():
                sent(ZM, zd)

            return 0

        lax.fori_loop(0, NZ, step, 0)

        @pl.when(z + EXPRESS < NZ)
        def _():
            sent(XP, z + EXPRESS)

        @pl.when(z - EXPRESS >= 0)
        def _():
            sent(XM, z - EXPRESS)

    def w1_copy(h, d):
        yd = wrap(y + d, NY)
        return remote(wp.at[h, yd], r1.at[h, pl.ds(y * 32, 32)], w1_s.at[h, d - 1], w1_r.at[h, d - 1], to_y(yd))

    def w1_start(h):
        for d in range(1, NY):
            w1_copy(h, d).start()

    def w1_wait(h):
        for d in range(1, NY):
            rows = pl.ds(wrap(y - d, NY) * 32, 32)
            remote(wp.at[h, 0], r1.at[h, rows], w1_s.at[h, d - 1], w1_r.at[h, d - 1], to_y(y_up)).wait_recv()

    def turn(h):
        turned = r1[h].astype(jnp.float32).T.astype(jnp.bfloat16)
        tt[h] = turned.reshape(3, NX, PART, 128)

    def w2_copy(h, d):
        xd = wrap(x + d, NX)
        return remote(tt.at[h, :, xd], r2.at[h, x], w2_s.at[h, d - 1], w2_r.at[h, d - 1], to_x(xd))

    def w2_start(h):
        for d in range(1, NX):
            w2_copy(h, d).start()
        r2[h, x] = tt[h, :, x]

    def w2_wait(h):
        for d in range(1, NX):
            xs = wrap(x - d, NX)
            remote(r2.at[h, 0], r2.at[h, xs], w2_s.at[h, d - 1], w2_r.at[h, d - 1], to_x(x_up)).wait_recv()

    def part_rows(p):
        return pl.ds(pl.multiple_of(p * PART, 16), PART)

    def w3_block(m, at):
        return wh.at[m, part_rows(x), pl.ds(pl.multiple_of(at * 128, 128), 128)]

    def w3_target(i):
        return lax.rem(i, 2) * NZ + (i // 2) * 2 + core

    def w3_copy(m, i):
        src = r2.at[m // 3, i // 2, m % 3]
        return remote(src, w3_block(m, zz), w3_s.at[m, i], w3_r.at[m, zz], to_zz(w3_target(i)))

    def w3_local(m, i):
        return pltpu.make_async_copy(r2.at[m // 3, i // 2, m % 3], w3_block(m, zz), w3_s.at[m, i])

    def w3_each(m, f_local, f_remote):
        def step(i, _):
            @pl.when(w3_target(i) == zz)
            def _():
                f_local(w3_local(m, i))

            @pl.when(w3_target(i) != zz)
            def _():
                f_remote(w3_copy(m, i))

            return 0

        lax.fori_loop(0, 2 * NX, step, 0)

    def w3_start(m):
        w3_each(m, lambda c: c.start(), lambda c: c.start())

    def w3_arrive(m):
        def step(i, _):
            @pl.when(i != zz)
            def _():
                remote(r2.at[0, 0, 0], w3_block(m, i), w3_s.at[m, 0], w3_r.at[m, i], sibling).wait_recv()

            return 0

        lax.fori_loop(0, NG * NZ, step, 0)

    def w4_copy(m, kind, p, g, to):
        blk = wh.at[m, part_rows(p), pl.ds(g * GCOL, GCOL)]
        return remote(blk, blk, w4_s.at[m, kind, g], w4_r.at[m, kind, g], to)

    def w5_copy(m, kind, p):
        blk = wh.at[m, part_rows(p)]
        return remote(blk, blk, w5_s.at[m, kind], w5_r.at[m, kind], sibling)

    hub = core == lax.rem(z, 2)
    parts = ((0, x), (1, x_down), (2, x_up), (3, x_far))

    def w4_send(m):
        w3_each(m, lambda c: c.wait(), lambda c: c.wait_send())

        @pl.when(hub)
        def _():
            w3_arrive(m)
            for g in range(NGRP):
                w4_copy(m, 0, x, g, to_x(x_up)).start()
                w4_copy(m, 1, x, g, to_x(x_down)).start()
            w5_copy(m, 0, x).start()

    def w4_relay(m):
        @pl.when(hub)
        def _():
            for g in range(NGRP):
                w4_copy(m, 0, x_down, g, to_x(x_up)).wait_recv()
                if g % 2 == 0:
                    w4_copy(m, 2, x_down, g, to_x(x_up)).start()
                w4_copy(m, 1, x_up, g, to_x(x_down)).wait_recv()
                if g % 2 == 1:
                    w4_copy(m, 2, x_up, g, to_x(x_down)).start()
            w5_copy(m, 1, x_down).start()
            w5_copy(m, 2, x_up).start()

    def w5_send(m):
        @pl.when(hub)
        def _():
            for g in range(NGRP):
                w4_copy(m, 2, x_far, g, to_x(x_up)).wait_recv()
            w5_copy(m, 3, x_far).start()

    def w5_wait(m):
        @pl.when(jnp.logical_not(hub))
        def _():
            for kind, p in parts:
                w5_copy(m, kind, p).wait_recv()

    def w_drain():
        @pl.when(hub)
        def _():
            for m in range(6):
                for kind, p in parts:
                    w5_copy(m, kind, p).wait_send()
                for kind in range(3):
                    for g in range(NGRP):
                        w4_copy(m, kind, x, g, to_x(x_up)).wait_send()

    def out_copy(m):
        return pltpu.make_async_copy(wh.at[m, pl.ds(0, WIDTH)], outs[m], out_s.at[m])

    def products(h, buf, part):
        whole = buf[...].reshape(D, TOK)
        wide = whole.astype(jnp.float32)
        squares = jnp.sum(wide * wide, axis=0, keepdims=True)
        row_scale = lax.rsqrt(squares / D + norm_eps) * D ** (-0.5)
        g = jnp.dot(wh[3 * h, 0:WIDTH], whole, preferred_element_type=jnp.float32) * row_scale
        u = jnp.dot(wh[3 * h + 1, 0:WIDTH], whole, preferred_element_type=jnp.float32) * row_scale
        hidden = (g / (1.0 + jnp.exp(-g)) * u).astype(jnp.bfloat16)

        def step(zd, _):
            w = wh[3 * h + 2, 0:WIDTH, pl.ds(pl.multiple_of(zd * 256, 256), 256)]
            p = lax.dot_general(w, hidden, (((0,), (0,)), ((), ())), preferred_element_type=jnp.float32)
            part[zd] = p.astype(jnp.bfloat16).reshape(NY, FEAT, TOK)
            return 0

        lax.fori_loop(0, NZ, step, 0)

    w1_start(0)
    gather_rounds(0, xa, 0, 1)
    w1_start(1)
    w1_wait(0)
    turn(0)
    w2_start(0)
    gather_rounds(0, xa, 1, 2)
    w2_wait(0)
    for m in range(3):
        w3_start(m)
    gather_rounds(0, xa, 2, 3)
    w1_wait(1)
    turn(1)
    w2_start(1)
    gather_rounds(0, xa, 3, STEPS)
    w4_send(0)
    gather_rounds(0, xa, STEPS, STEPS + LAG)
    w4_send(1)
    w4_relay(0)
    w4_send(2)
    w4_relay(1)
    w5_send(0)
    gather_end(0, xa)
    w4_relay(2)
    w5_send(1)
    w5_send(2)
    w2_wait(1)
    for m in range(3, 6):
        w3_start(m)
    for m in range(3):
        w5_wait(m)
    for m in range(3):
        out_copy(m).start()
    products(0, xa, pa)
    xb[z, y] = sum_result(0, pa, ra, xa[z, y])
    gather_rounds(1, xb, 0, 1)
    for m in range(3, 6):
        w4_send(m)
    gather_rounds(1, xb, 1, 3)
    for m in range(3, 6):
        w4_relay(m)
    gather_rounds(1, xb, 3, STEPS)
    for m in range(3, 6):
        w5_send(m)
    gather_rounds(1, xb, STEPS, STEPS + LAG)
    gather_end(1, xb)
    for m in range(3, 6):
        w5_wait(m)
    for m in range(3, 6):
        out_copy(m).start()
    products(1, xb, pb)
    res_ref[...] = sum_result(1, pb, rb, xb[z, y])

    for h in range(2):
        for d in range(1, 4):
            w1_copy(h, d).wait_send()
            w2_copy(h, d).wait_send()
    w_drain()
    for m in range(6):
        out_copy(m).wait()
    gather_drain(0, xa)
    gather_drain(1, xb)
    sum_drain(0, pa, ra)
    sum_drain(1, pb, rb)


def write_out(*refs):
    ins, outs, held, sems = refs[:7], refs[7:14], refs[14:21], refs[21]
    loads = [pltpu.make_async_copy(ins[i], held[i], sems.at[0, i]) for i in range(7)]
    stores = [pltpu.make_async_copy(held[i], outs[i], sems.at[1, i]) for i in range(7)]
    for c in loads:
        c.start()
    for i in range(7):
        loads[i].wait()
        stores[i].start()
    for c in stores:
        c.wait()


def local(prompt, gain_pre, gate_pre, up_pre, down_pre, gain_post, gate_post, up_post, down_post):
    vm = pl.BlockSpec(memory_space=pltpu.VMEM)
    dma = pltpu.SemaphoreType.DMA
    bf = jnp.bfloat16
    hbm = pl.BlockSpec(memory_space=pltpu.HBM)
    shapes = (jax.ShapeDtypeStruct((FEAT, TOK), bf),) + (jax.ShapeDtypeStruct((WIDTH, D), bf),) * 6
    made = pl.pallas_call(
        kernel,
        out_shape=shapes,
        in_specs=[hbm] * 9,
        out_specs=(vm,) + (hbm,) * 6,
        scratch_shapes=[
            pltpu.VMEM((NZ, NY, FEAT, TOK), bf),
            pltpu.VMEM((NZ, NY, FEAT, TOK), bf),
            pltpu.VMEM((NZ, NY, FEAT, TOK), bf),
            pltpu.VMEM((NZ, NY, FEAT, TOK), bf),
            pltpu.VMEM((7, NZ, FEAT, TOK), bf),
            pltpu.VMEM((7, NZ, FEAT, TOK), bf),
            pltpu.VMEM((2, NY, 32, 3 * ROWS), bf),
            pltpu.VMEM((2, 128, 3 * ROWS), bf),
            pltpu.VMEM((2, 3, NX, PART, 128), bf),
            pltpu.VMEM((2, NX, 3, PART, 128), bf),
            pltpu.VMEM((6, ROWS, D), bf),
            pltpu.VMEM((2, 1, 32), jnp.float32),
            pltpu.VMEM((6, 32, NY * WIDTH), jnp.float32),
            dma((2, 7, NZ)),
            dma((2, 7, NZ)),
            dma((2, 7, NZ)),
            dma((2, 7, NZ)),
            dma((2, 3)),
            dma((2, 3)),
            dma((2, 3)),
            dma((2, 3)),
            dma((6, 2 * NX)),
            dma((6, NG * NZ)),
            dma((6, 3, NGRP)),
            dma((6, 3, NGRP)),
            dma((6, 4)),
            dma((6, 4)),
            dma((9,)),
            dma((6,)),
        ],
        compiler_params=pltpu.CompilerParams(
            collective_id=0, has_side_effects=True, vmem_limit_bytes=58 * 1024 * 1024
        ),
    )(
        prompt.T,
        gain_pre.reshape(1, 32),
        gain_post.reshape(1, 32),
        gate_pre,
        up_pre,
        down_pre,
        gate_post,
        up_post,
        down_post,
    )
    res, *served = pl.pallas_call(
        write_out,
        out_shape=shapes,
        in_specs=[hbm] * 7,
        out_specs=(hbm,) * 7,
        scratch_shapes=[pltpu.VMEM(a.shape, bf) for a in shapes] + [dma((2, 7))],
    )(*made)
    return (res.T, *served)


def solution(mesh):
    rows = P(("gr", "fs"))
    block = P(("gr", "fs"), "tp")
    tokens = P(("gr", "tp"), "fs")
    return jax.shard_map(
        local,
        mesh=mesh,
        in_specs=(tokens, rows, block, block, block, rows, block, block, block),
        out_specs=(tokens,) + (P("fs", None),) * 6,
        check_vma=False,
    )
```

time: 1140 us -> 163 us (0.14)
  waiting for transfers between devices: 1000 us -> 0 us
  Pallas kernels: 0 us -> 162 us
  blocking collectives: 51.3 us -> 0 us
  local copies, waits for them, and re-layouts: 50 us -> 0 us
  between operations: 14 us -> 0.64 us
  matrix products: 12.1 us -> 0 us
    all_gather x3 -> x0, waiting for transfers between devices: 525 us -> none  [the longest x2 379 us: half_step(): whole = lax.all_gather(tokens_t, 'fs', axis=0, tiled=True)]
    reduce_scatter x2 -> x0, waiting for transfers between devices: 475 us -> none  [half_step(): lax.psum_scatter(partial_value.astype(jnp.bfloat16), 'fs', scatter_dimens...]
    pallas_call x0 -> x2, Pallas kernels: none -> 162 us  [the longest x1 159 us: local(): pl.pallas_call(kernel, out_shape=shapes, in_specs=[hbm] * 9, out_specs=(v...]
    all_to_all x2 -> x0, blocking collectives: 51.3 us -> none  [the longest x1 37.3 us: relayout(): m = lax.all_to_all(m, 'fs', 0, 0, tiled=True)]
    slice x7 -> x0, local copies, waits for them, and re-layouts: 17.8 us -> none  [relayout(): return tuple((m[i] for i in range(6)))]
    squeeze x6 -> x0, local copies, waits for them, and re-layouts: 12.6 us -> none  [relayout(): return tuple((m[i] for i in range(6)))]
    dot_general x4 -> x0, matrix products: 12.1 us -> none  [the longest x2 9 us: half_step(): lax.dot_general(w_down, hidden, (((0,), (0,)), ((), ())), preferred_eleme...]
  transfers between devices with their start and end apart: 5 -> 0, of which waited for: 5 -> 0; matrix products, arithmetic and copies ran while one was open for 2% -> 0% of each run, Pallas kernels for 0% -> 0%
where the time goes in v3:
time: 163 us
  Pallas kernels  162 us (99%)
    pallas_call x1, Pallas kernels, local(): pl.pallas_call(kernel, out_shape=shapes, in_specs=[hbm] * 9, out_specs=(v...  159 us
    pallas_call x1, Pallas kernels, local(): pl.pallas_call(write_out, out_shape=shapes, in_specs=[hbm] * 7, out_specs...  3.71 us

profile of v3, /device:TPU:6, one launch (start us, length us, event | category | flops | bytes accessed | tf_op | source)
XLA Modules:
  0.0 163.0 jit_solution(2773543140684429866)
XLA Ops:
  0.6 158.7 %shard_map.144 = (bf16[64,512]{1,0:T(8,128)(2,1)}, bf16[176,2048]{1,0:T(8,128)(2,1)}, bf16[176,2048]{1,0:T(8,128)(2,1)}, bf16[176,2048]{1,0:T(8,128)(2,1)}, bf16...) custom-call(bf16[64,512]{1,0:T(8,128)(2,1)} %bitcast.4, f32[1,32]{1,0:T(1,128)} %bitcast.5, ...), custom_call_target="tpu_custom_call" | custom-call | tf_op jit(solution)/shard_map/pallas_call | solution.py:576
  159.3 3.7 %shard_map.145 = (bf16[64,512]{1,0:T(8,128)(2,1)}, bf16[176,2048]{1,0:T(8,128)(2,1)}, bf16[176,2048]{1,0:T(8,128)(2,1)}, bf16[176,2048]{1,0:T(8,128)(2,1)}, bf16...) custom-call(bf16[64,512]{1,0:T(8,128)(2,1)} %get-tuple-element.21.refs_0_, ...), custom_call_target="tpu_custom_call" | custom-call | tf_op jit(solution)/shard_map/pallas_call | solution.py:626

commit v4 on v3

v4 whole, which is shorter than its diff:
```python
import jax
import jax.numpy as jnp
from jax import lax
from jax.experimental import pallas as pl
from jax.experimental.pallas import tpu as pltpu
from jax.sharding import PartitionSpec as P

D = 2048
FF = 5632
NX, NY, NZ, NG = 4, 4, 8, 2
WIDTH = 176
FEAT = 64
TOK = 512
PART = 48
ROWS = NX * PART
NGRP = 2
GCOL = D // NGRP
EXPRESS = 4

norm_eps = 1e-06
MESH = pl.DeviceIdType.MESH


def kernel(
    x_ref, gain_a, gain_b, *refs
):
    mats, res_ref, outs = refs[:6], refs[6], refs[7:13]
    (xa, xb, pa, pb, ra, rb, wp, r1, tt, r2, wh, gains, loaded, hid) = refs[13:27]
    (ag_s, ag_r, rs_s, rs_r, w1_s, w1_r, w2_s, w2_r, w3_s, w3_r, w4_s, w4_r, w5_s, w5_r, in_s, out_s) = refs[27:]
    HALVES = [(c, pl.ds(32 * c, 32)) for c in range(2)]

    gr, fs, tp = lax.axis_index("gr"), lax.axis_index("fs"), lax.axis_index("tp")
    y, z = lax.rem(fs, NY), fs // NY
    core, x = lax.rem(tp, 2), tp // 2
    zz = gr * NZ + z

    loads = [pltpu.make_async_copy(m, loaded.at[i], in_s.at[i]) for i, m in enumerate(mats)]
    loads.append(pltpu.make_async_copy(gain_a, gains.at[0], in_s.at[6]))
    loads.append(pltpu.make_async_copy(gain_b, gains.at[1], in_s.at[7]))
    loads.append(pltpu.make_async_copy(x_ref, xa.at[z, y], in_s.at[8]))
    for c in loads:
        c.start()

    def wrap(v, n):
        return lax.rem(v + n, n)

    def to_y(v):
        return {"fs": z * NY + v}

    def to_z(v):
        return {"fs": v * NY + y}

    def to_zz(v):
        return {"gr": v // NZ, "fs": lax.rem(v, NZ) * NY + y}

    def to_x(v):
        return {"tp": v * 2 + core}

    sibling = {"tp": x * 2 + 1 - core}
    y_up, y_down, y_far = wrap(y + 1, NY), wrap(y - 1, NY), wrap(y + 2, NY)
    x_up, x_down, x_far = wrap(x + 1, NX), wrap(x - 1, NX), wrap(x + 2, NX)

    def remote(src, dst, s, r, to):
        return pltpu.make_async_remote_copy(src, dst, s, r, device_id=to, device_id_type=MESH)

    barrier = pltpu.get_barrier_semaphore()

    def greet_z(i, _):
        pl.semaphore_signal(barrier, inc=1, device_id=to_zz(lax.rem(zz + i, NG * NZ)), device_id_type=MESH)
        return 0

    lax.fori_loop(1, NG * NZ, greet_z, 0)
    for d in range(1, 4):
        pl.semaphore_signal(barrier, inc=1, device_id=to_y(wrap(y + d, NY)), device_id_type=MESH)
        pl.semaphore_signal(barrier, inc=1, device_id=to_x(wrap(x + d, NX)), device_id_type=MESH)
    pl.semaphore_signal(barrier, inc=1, device_id=sibling, device_id_type=MESH)

    def pack(h):
        eye = lax.broadcasted_iota(jnp.int32, (32, 32), 0) == lax.broadcasted_iota(jnp.int32, (32, 32), 1)
        gain = jnp.sum(jnp.where(eye, jnp.broadcast_to(gains[h], (32, 32)), 0.0), axis=1, keepdims=True)
        for m in range(3):
            v = loaded[h * 3 + m]
            v = v * gain if m < 2 else v
            for at in range(NY):
                piece = jnp.pad(v[:, at * WIDTH : (at + 1) * WIDTH], ((0, 0), (0, ROWS - WIDTH)))
                wp[h, at, :, m * ROWS : (m + 1) * ROWS] = piece.astype(jnp.bfloat16)

    for c in loads:
        c.wait()
    pack(0)
    pack(1)
    for h in range(2):
        r1[h, pl.ds(y * 32, 32), :] = wp[h, y]
    pl.semaphore_wait(barrier, NG * NZ - 1 + 3 + 3 + 1)

    STEPS = 6

    def each(s, f_low, f_high):
        d1 = s + jnp.where(s >= 4, 2, 0)
        fits = (s >= 0) & (s < STEPS)

        @pl.when(fits & (z - d1 >= 0))
        def _():
            f_low(z - d1, d1)

        @pl.when(fits & (d1 > 0) & (z + d1 < NZ))
        def _():
            f_high(z + d1, d1)

        d2 = s + 2
        second = (s == 2) | (s == 3)

        @pl.when(second & (z - d2 >= 0))
        def _():
            f_low(z - d2, d2)

        @pl.when(second & (z + d2 < NZ))
        def _():
            f_high(z + d2, d2)

    z_up, z_down = jnp.minimum(z + 1, NZ - 1), jnp.maximum(z - 1, 0)
    z_far_up, z_far_down = jnp.minimum(z + EXPRESS, NZ - 1), jnp.maximum(z - EXPRESS, 0)

    def gather_copy(k, buf, zs, ys, half, link, arrival, to):
        blk = buf.at[zs, ys, half]
        return remote(blk, blk, ag_s.at[k, link], ag_r.at[k, arrival], to)

    DIRECT, RELAYED, UPWARD, DOWNWARD = 16, 17, 18, 34

    def even(v):
        return lax.rem(v, 2) == 0

    def arrived(k, buf, zs, half, arrival):
        gather_copy(k, buf, zs, y, half, 0, arrival, to_y(y_up)).wait_recv()

    def along_y(k, buf, zs, c, half):
        up = jnp.where(even(zs), 2 * zs + c, DIRECT)
        down = jnp.where(even(zs), DIRECT, 2 * zs + c)
        gather_copy(k, buf, zs, y, half, 0, up, to_y(y_up)).start()
        gather_copy(k, buf, zs, y, half, 0, down, to_y(y_down)).start()

    def gather_low(k, buf, zs, d):
        for c, half in HALVES:
            up, down = UPWARD + 2 * zs + c, DOWNWARD + 2 * zs + c

            @pl.when(d > 0)
            def _():
                arrived(k, buf, zs, half, up)

            @pl.when((z < NZ - 1) & (d != EXPRESS - 1))
            def _():
                gather_copy(k, buf, zs, y, half, 1, up, to_z(z_up)).start()

            @pl.when((d == 0) & (z > 0))
            def _():
                gather_copy(k, buf, zs, y, half, 1, down, to_z(z_down)).start()

            @pl.when((d == 0) & (z + EXPRESS < NZ))
            def _():
                gather_copy(k, buf, zs, y, half, 1, up, to_z(z_far_up)).start()

            @pl.when((d == 0) & (z - EXPRESS >= 0))
            def _():
                gather_copy(k, buf, zs, y, half, 1, down, to_z(z_far_down)).start()

            along_y(k, buf, zs, c, half)

    def gather_high(k, buf, zs, d):
        for c, half in HALVES:
            down = DOWNWARD + 2 * zs + c
            arrived(k, buf, zs, half, down)

            @pl.when((z > 0) & (d != EXPRESS - 1))
            def _():
                gather_copy(k, buf, zs, y, half, 1, down, to_z(z_down)).start()

            along_y(k, buf, zs, c, half)

    def gather_relay(k, buf, zs):
        origin = jnp.where(even(zs), y_down, y_up)
        onward = jnp.where(even(zs), y_up, y_down)
        for c, half in HALVES:
            arrived(k, buf, zs, half, 2 * zs + c)
            gather_copy(k, buf, zs, origin, half, 0, RELAYED, to_y(onward)).start()

    LAG = 2

    def gather_rounds(k, buf, first, last):
        def step(s, _):
            each(s, lambda zs, d: gather_low(k, buf, zs, d), lambda zs, d: gather_high(k, buf, zs, d))
            each(s - LAG, lambda zs, d: gather_relay(k, buf, zs), lambda zs, d: gather_relay(k, buf, zs))
            return 0

        lax.fori_loop(first, last, step, 0)

    def gather_end(k, buf):
        for arrival in (DIRECT, RELAYED):
            blocks = buf.at[:, y_far]
            remote(blocks, blocks, ag_s.at[k, 0], ag_r.at[k, arrival], to_y(y_up)).wait_recv()

    def wait_sent(sem, blocks):
        remote(blocks, blocks, sem, ag_r.at[0, 0], to_y(y_up)).wait_send()

    def gather_drain(k):
        wait_sent(ag_s.at[k, 0], ra.at[0:3])

        @pl.when((z == 0) | (z == 7))
        def _():
            wait_sent(ag_s.at[k, 1], ra.at[0, 0:2])

        @pl.when((z == 3) | (z == 4))
        def _():
            wait_sent(ag_s.at[k, 1], ra.at[0])

        @pl.when((z == 1) | (z == 2) | (z == 5) | (z == 6))
        def _():
            wait_sent(ag_s.at[k, 1], ra.at[0:3, 0:3])

    FAR, UP, DN, ZP, ZM, XP, XM = range(7)
    BOTH, CHAIN_UP, CHAIN_DOWN, FAR_UP, FAR_DOWN = 16, 32, 48, 64, 66

    def send_part(k, part, land, zd, col, half, link, kind, arrival, to):
        return remote(part.at[zd, col, half], land.at[kind, zd, half], rs_s.at[k, link], rs_r.at[k, arrival], to)

    def landed(k, land, kind, zd, half, arrival):
        blk = land.at[kind, zd] if half is None else land.at[kind, zd, half]
        remote(blk, blk, rs_s.at[k, 0], rs_r.at[k, arrival], to_y(y_up)).wait_recv()

    def wide(v):
        return v.astype(jnp.float32)

    def sum_far(k, part, land, zd):
        onward = jnp.where(even(zd), y_up, y_down)
        direct = jnp.where(even(zd), y_down, y_up)
        place = jnp.where(even(zd), DN, UP)
        for c, half in HALVES:
            send_part(k, part, land, zd, y_far, half, 0, FAR, 2 * zd + c, to_y(onward)).start()
            send_part(k, part, land, zd, direct, half, 0, place, BOTH + 2 * zd + c, to_y(direct)).start()

    def sum_near(k, part, land, zd):
        target = jnp.where(even(zd), y_up, y_down)
        place = jnp.where(even(zd), UP, DN)
        for c, half in HALVES:
            landed(k, land, FAR, zd, half, 2 * zd + c)
            part[zd, target, half] = (wide(part[zd, target, half]) + wide(land[FAR, zd, half])).astype(jnp.bfloat16)
            send_part(k, part, land, zd, target, half, 0, place, BOTH + 2 * zd + c, to_y(target)).start()

    def column_sum(k, part, land, zd, c, half):
        landed(k, land, UP, zd, None, BOTH + 2 * zd + c)
        return wide(part[zd, y, half]) + wide(land[UP, zd, half]) + wide(land[DN, zd, half])

    def sum_along_z(k, part, land, zd, d, chain, arrival, express, far_arrival, more, to_next, to_far):
        for c, half in HALVES:
            own = column_sum(k, part, land, zd, c, half)
            chained = more & (d != EXPRESS - 1)

            @pl.when(jnp.logical_not(chained))
            def _():
                part[zd, y, half] = own.astype(jnp.bfloat16)

            @pl.when(chained)
            def _():
                landed(k, land, chain, zd, half, arrival + 2 * zd + c)
                part[zd, y, half] = (own + wide(land[chain, zd, half])).astype(jnp.bfloat16)

            @pl.when(d != EXPRESS)
            def _():
                send_part(k, part, land, zd, y, half, 1, chain, arrival + 2 * zd + c, to_next).start()

            @pl.when(d == EXPRESS)
            def _():
                send_part(k, part, land, zd, y, half, 1, express, far_arrival + c, to_far).start()

    def sum_upward(k, part, land, zd, d):
        sum_along_z(k, part, land, zd, d, ZP, CHAIN_UP, XP, FAR_UP, z > 0, to_z(z_up), to_z(z_far_up))

    def sum_downward(k, part, land, zd, d):
        @pl.when(d > 0)
        def _():
            more = z < NZ - 1
            sum_along_z(k, part, land, zd, d, ZM, CHAIN_DOWN, XM, FAR_DOWN, more, to_z(z_down), to_z(z_far_down))

    def sum_result(k, part, land, own, give):
        def step(i, _):
            s = STEPS - 1 - i
            each(s, lambda zd, d: sum_far(k, part, land, zd), lambda zd, d: sum_far(k, part, land, zd))
            each(s + 1, lambda zd, d: sum_near(k, part, land, zd), lambda zd, d: sum_near(k, part, land, zd))
            each(
                s + 2,
                lambda zd, d: sum_downward(k, part, land, zd, d),
                lambda zd, d: sum_upward(k, part, land, zd, d),
            )
            return 0

        lax.fori_loop(0, STEPS + 1, step, 0)
        for c, half in HALVES:
            total = column_sum(k, part, land, z, c, half)
            for kind, there, arrival in (
                (ZP, z > 0, CHAIN_UP + 2 * z + c),
                (ZM, z < NZ - 1, CHAIN_DOWN + 2 * z + c),
                (XP, z - EXPRESS >= 0, FAR_UP + c),
                (XM, z + EXPRESS < NZ, FAR_DOWN + c),
            ):

                @pl.when(there)
                def _():
                    landed(k, land, kind, z, half, arrival)

                @pl.when(jnp.logical_not(there))
                def _():
                    land[kind, z, half] = jnp.zeros((32, TOK), jnp.bfloat16)

                total = total + wide(land[kind, z, half])
            give(half, (wide(own(half)) + 0.5 * FF ** (-0.5) * total).astype(jnp.bfloat16))

    def sum_drain(k, land):
        wait_sent(rs_s.at[k, 0], land.at[0:3])
        wait_sent(rs_s.at[k, 1], land.at[0, 0:7])

    def w1_copy(h, d):
        yd = wrap(y + d, NY)
        return remote(wp.at[h, yd], r1.at[h, pl.ds(y * 32, 32)], w1_s.at[h], w1_r.at[h], to_y(yd))

    def w1_start(h):
        for d in range(1, NY):
            w1_copy(h, d).start()

    def w1_wait(h):
        rows = r1.at[h, 0:96]
        remote(rows, rows, w1_s.at[h], w1_r.at[h], to_y(y_up)).wait_recv()

    def turn(h):
        turned = r1[h].astype(jnp.float32).T.astype(jnp.bfloat16)
        tt[h] = turned.reshape(3, NX, PART, 128)

    def w2_start(h):
        for d in range(1, NX):
            xd = wrap(x + d, NX)
            remote(tt.at[h, :, xd], r2.at[h, x], w2_s.at[h], w2_r.at[h], to_x(xd)).start()
        r2[h, x] = tt[h, :, x]

    def w2_wait(h):
        three = r2.at[h, 0:3]
        remote(three, three, w2_s.at[h], w2_r.at[h], to_x(x_up)).wait_recv()

    hub = core == lax.rem(z, 2)

    def part_rows(p):
        return pl.ds(pl.multiple_of(p * PART, 16), PART)

    def w3_columns():
        return pl.ds(pl.multiple_of(zz * 128, 128), 128)

    def w3_start(m):
        def step(i, _):
            target = lax.rem(i, 2) * NZ + (i // 2) * 2 + core

            @pl.when(target == zz)
            def _():
                wh[m, part_rows(x), w3_columns()] = r2[m // 3, i // 2, m % 3]

            @pl.when(target != zz)
            def _():
                block = wh.at[m, part_rows(x), w3_columns()]
                remote(r2.at[m // 3, i // 2, m % 3], block, w3_s.at[m // 3], w3_r.at[m], to_zz(target)).start()

            return 0

        lax.fori_loop(0, 2 * NX, step, 0)

    def w3_drain(h):
        @pl.when(hub)
        def _():
            wait_sent(w3_s.at[h], wh.at[0, 0 : 3 * PART, 0 : 7 * 128])

        @pl.when(jnp.logical_not(hub))
        def _():
            wait_sent(w3_s.at[h], wh.at[0, 0 : 3 * PART, 0 : 8 * 128])

    def w4_copy(m, kind, p, g, to):
        blk = wh.at[m, part_rows(p), pl.ds(g * GCOL, GCOL)]
        return remote(blk, blk, w4_s.at[0], w4_r.at[m, 4 if kind == 2 else 2 * kind + g], to)

    def w5_copy(m, p):
        blk = wh.at[m, part_rows(p)]
        return remote(blk, blk, w5_s.at[0], w5_r.at[m], sibling)

    def w4_send(m):
        @pl.when(hub)
        def _():
            others = wh.at[m, 0:PART, 0 : 15 * 128]
            remote(others, others, w3_s.at[0], w3_r.at[m], sibling).wait_recv()
            for g in range(NGRP):
                w4_copy(m, 0, x, g, to_x(x_up)).start()
                w4_copy(m, 1, x, g, to_x(x_down)).start()
            w5_copy(m, x).start()

    def w4_relay(m):
        @pl.when(hub)
        def _():
            for g in range(NGRP):
                w4_copy(m, 0, x_down, g, to_x(x_up)).wait_recv()
                if g % 2 == 0:
                    w4_copy(m, 2, x_down, g, to_x(x_up)).start()
                w4_copy(m, 1, x_up, g, to_x(x_down)).wait_recv()
                if g % 2 == 1:
                    w4_copy(m, 2, x_up, g, to_x(x_down)).start()
            w5_copy(m, x_down).start()
            w5_copy(m, x_up).start()

    def w5_send(m):
        @pl.when(hub)
        def _():
            far = wh.at[m, part_rows(x_far)]
            remote(far, far, w4_s.at[0], w4_r.at[m, 4], sibling).wait_recv()
            w5_copy(m, x_far).start()

    def w5_wait(m):
        @pl.when(jnp.logical_not(hub))
        def _():
            remote(wh.at[m], wh.at[m], w5_s.at[0], w5_r.at[m], sibling).wait_recv()

    def w_drain():
        for h in range(2):
            wait_sent(w1_s.at[h], wp.at[h, 0:3])
            wait_sent(w2_s.at[h], r2.at[h, 0:3])
            w3_drain(h)

        @pl.when(hub)
        def _():
            wait_sent(w4_s.at[0], wh.at[:, 0 : 3 * PART])
            wait_sent(w5_s.at[0], wh)

    def out_copy(m):
        return pltpu.make_async_copy(wh.at[m, pl.ds(0, WIDTH)], outs[m], out_s.at[m])

    def hidden_units(h, buf):
        whole = buf[...].reshape(D, TOK)
        wide_whole = whole.astype(jnp.float32)
        squares = jnp.sum(wide_whole * wide_whole, axis=0, keepdims=True)
        row_scale = lax.rsqrt(squares / D + norm_eps) * D ** (-0.5)
        g = jnp.dot(wh[3 * h, 0:WIDTH], whole, preferred_element_type=jnp.float32) * row_scale
        u = jnp.dot(wh[3 * h + 1, 0:WIDTH], whole, preferred_element_type=jnp.float32) * row_scale
        hid[...] = (g / (1.0 + jnp.exp(-g)) * u).astype(jnp.bfloat16)

    def partial_sums(h, part):
        def step(zd, _):
            w = wh[3 * h + 2, 0:WIDTH, pl.ds(pl.multiple_of(zd * 256, 256), 256)]
            p = lax.dot_general(w, hid[...], (((0,), (0,)), ((), ())), preferred_element_type=jnp.float32)
            part[zd] = p.astype(jnp.bfloat16).reshape(NY, FEAT, TOK)
            return 0

        lax.fori_loop(0, NZ, step, 0)

    w1_start(0)
    gather_rounds(0, xa, 0, 1)
    w1_start(1)
    gather_rounds(0, xa, 1, 2)
    w1_wait(0)
    turn(0)
    w2_start(0)
    gather_rounds(0, xa, 2, 3)
    w2_wait(0)
    for m in range(3):
        w3_start(m)
    gather_rounds(0, xa, 3, 5)
    w4_send(0)
    w1_wait(1)
    turn(1)
    w2_start(1)
    gather_rounds(0, xa, 5, 6)
    w4_relay(0)
    w4_send(1)
    gather_rounds(0, xa, 6, 7)
    w4_send(2)
    w4_relay(1)
    w5_send(0)
    gather_rounds(0, xa, 7, 8)
    w4_relay(2)
    w5_send(1)
    gather_end(0, xa)
    w5_send(2)
    w2_wait(1)
    for m in range(3, 6):
        w3_start(m)
    for m in range(2):
        w5_wait(m)
    hidden_units(0, xa)
    w5_wait(2)
    for m in range(3):
        out_copy(m).start()
    partial_sums(0, pa)

    def keep_middle(half, value):
        xb[z, y, half] = value

    def keep_result(half, value):
        res_ref[half] = value

    sum_result(0, pa, ra, lambda half: xa[z, y, half], keep_middle)
    gather_rounds(1, xb, 0, 1)
    for m in range(3, 6):
        w4_send(m)
    gather_rounds(1, xb, 1, 3)
    for m in range(3, 6):
        w4_relay(m)
    gather_rounds(1, xb, 3, STEPS)
    for m in range(3, 6):
        w5_send(m)
    gather_rounds(1, xb, STEPS, STEPS + LAG)
    gather_end(1, xb)
    for m in range(3, 6):
        w5_wait(m)
    for m in range(3, 6):
        out_copy(m).start()
    hidden_units(1, xb)
    partial_sums(1, pb)
    sum_result(1, pb, rb, lambda half: xb[z, y, half], keep_result)

    w_drain()
    for m in range(6):
        out_copy(m).wait()
    for k, land in ((0, ra), (1, rb)):
        gather_drain(k)
        sum_drain(k, land)


def write_out(*refs):
    ins, outs, held, sems = refs[:7], refs[7:14], refs[14:21], refs[21]
    loads = [pltpu.make_async_copy(ins[i], held[i], sems.at[0, i]) for i in range(7)]
    stores = [pltpu.make_async_copy(held[i], outs[i], sems.at[1, i]) for i in range(7)]
    for c in loads:
        c.start()
    for i in range(7):
        loads[i].wait()
        stores[i].start()
    for c in stores:
        c.wait()


def local(prompt, gain_pre, gate_pre, up_pre, down_pre, gain_post, gate_post, up_post, down_post):
    vm = pl.BlockSpec(memory_space=pltpu.VMEM)
    dma = pltpu.SemaphoreType.DMA
    bf = jnp.bfloat16
    hbm = pl.BlockSpec(memory_space=pltpu.HBM)
    shapes = (jax.ShapeDtypeStruct((FEAT, TOK), bf),) + (jax.ShapeDtypeStruct((WIDTH, D), bf),) * 6
    made = pl.pallas_call(
        kernel,
        out_shape=shapes,
        in_specs=[hbm] * 9,
        out_specs=(vm,) + (hbm,) * 6,
        scratch_shapes=[
            pltpu.VMEM((NZ, NY, FEAT, TOK), bf),
            pltpu.VMEM((NZ, NY, FEAT, TOK), bf),
            pltpu.VMEM((NZ, NY, FEAT, TOK), bf),
            pltpu.VMEM((NZ, NY, FEAT, TOK), bf),
            pltpu.VMEM((7, NZ, FEAT, TOK), bf),
            pltpu.VMEM((7, NZ, FEAT, TOK), bf),
            pltpu.VMEM((2, NY, 32, 3 * ROWS), bf),
            pltpu.VMEM((2, 128, 3 * ROWS), bf),
            pltpu.VMEM((2, 3, NX, PART, 128), bf),
            pltpu.VMEM((2, NX, 3, PART, 128), bf),
            pltpu.VMEM((6, ROWS, D), bf),
            pltpu.VMEM((2, 1, 32), jnp.float32),
            pltpu.VMEM((6, 32, NY * WIDTH), jnp.float32),
            pltpu.VMEM((WIDTH, TOK), bf),
            dma((2, 2)),
            dma((2, 50)),
            dma((2, 2)),
            dma((2, 68)),
            dma((2,)),
            dma((2,)),
            dma((2,)),
            dma((2,)),
            dma((2,)),
            dma((6,)),
            dma((1,)),
            dma((6, 5)),
            dma((1,)),
            dma((6,)),
            dma((9,)),
            dma((6,)),
        ],
        compiler_params=pltpu.CompilerParams(
            collective_id=0, has_side_effects=True, vmem_limit_bytes=58 * 1024 * 1024
        ),
    )(
        prompt.T,
        gain_pre.reshape(1, 32),
        gain_post.reshape(1, 32),
        gate_pre,
        up_pre,
        down_pre,
        gate_post,
        up_post,
        down_post,
    )
    res, *served = pl.pallas_call(
        write_out,
        out_shape=shapes,
        in_specs=[hbm] * 7,
        out_specs=(hbm,) * 7,
        scratch_shapes=[pltpu.VMEM(a.shape, bf) for a in shapes] + [dma((2, 7))],
    )(*made)
    return (res.T, *served)


def solution(mesh):
    rows = P(("gr", "fs"))
    block = P(("gr", "fs"), "tp")
    tokens = P(("gr", "tp"), "fs")
    return jax.shard_map(
        local,
        mesh=mesh,
        in_specs=(tokens, rows, block, block, block, rows, block, block, block),
        out_specs=(tokens,) + (P("fs", None),) * 6,
        check_vma=False,
    )
```

time: 163 us -> 151 us (0.926)
  Pallas kernels: 162 us -> 149 us
    pallas_call x1, Pallas kernels: 159 us -> 145 us  [local(): pl.pallas_call(kernel, out_shape=shapes, in_specs=[hbm] * 9, out_specs=(v...]
where the time goes in v4:
time: 151 us; the launch traced here: 150 us
  Pallas kernels  149 us (99%)
    pallas_call x1, Pallas kernels, local(): pl.pallas_call(kernel, out_shape=shapes, in_specs=[hbm] * 9, out_specs=(v...  145 us
    pallas_call x1, Pallas kernels, local(): pl.pallas_call(write_out, out_shape=shapes, in_specs=[hbm] * 7, out_specs...  3.71 us

profile of v4, /device:TPU:6, one launch (start us, length us, event | category | flops | bytes accessed | tf_op | source)
XLA Modules:
  0.0 149.7 jit_solution(18039518900343652265)
XLA Ops:
  0.6 145.3 %shard_map.144 = (bf16[64,512]{1,0:T(8,128)(2,1)}, bf16[176,2048]{1,0:T(8,128)(2,1)}, bf16[176,2048]{1,0:T(8,128)(2,1)}, bf16[176,2048]{1,0:T(8,128)(2,1)}, bf16...) custom-call(bf16[64,512]{1,0:T(8,128)(2,1)} %bitcast.4, f32[1,32]{1,0:T(1,128)} %bitcast.5, ...), custom_call_target="tpu_custom_call" | custom-call | tf_op jit(solution)/shard_map/pallas_call | solution.py:547
  146.0 3.7 %shard_map.145 = (bf16[64,512]{1,0:T(8,128)(2,1)}, bf16[176,2048]{1,0:T(8,128)(2,1)}, bf16[176,2048]{1,0:T(8,128)(2,1)}, bf16[176,2048]{1,0:T(8,128)(2,1)}, bf16...) custom-call(bf16[64,512]{1,0:T(8,128)(2,1)} %get-tuple-element.21.refs_0_, ...), custom_call_target="tpu_custom_call" | custom-call | tf_op jit(solution)/shard_map/pallas_call | solution.py:598

commit v5 on v4

v5 whole, which is shorter than its diff:
```python
import jax
import jax.numpy as jnp
from jax import lax
from jax.experimental import pallas as pl
from jax.experimental.pallas import tpu as pltpu
from jax.sharding import PartitionSpec as P

D = 2048
FF = 5632
NX, NY, NZ, NG = 4, 4, 8, 2
WIDTH = 176
FEAT = 64
TOK = 512
STREAM = TOK // 2
OFFSET = 0
PART = 48
ROWS = NX * PART
NGRP = 2
GCOL = D // NGRP
STRIDE = 3

norm_eps = 1e-06
MESH = pl.DeviceIdType.MESH


def kernel(
    x_ref, gain_a, gain_b, *refs
):
    mats, res_ref, outs = refs[:6], refs[6], refs[7:13]
    (xs_ref, part, land, wp, r1, r2, wh, gains, loaded, hid) = refs[13:23]
    (ag_s, ag_r, rs_s, rs_r, w1_s, w1_r, w3_s, w3_r, w4_s, w4_r, w5_s, w5_r, in_s, out_s) = refs[23:]

    gr, fs, tp = lax.axis_index("gr"), lax.axis_index("fs"), lax.axis_index("tp")
    y, z = lax.rem(fs, NY), fs // NY
    core, x = lax.rem(tp, 2), tp // 2
    zz = gr * NZ + z

    loads = [pltpu.make_async_copy(m, loaded.at[i], in_s.at[i]) for i, m in enumerate(mats)]
    loads.append(pltpu.make_async_copy(gain_a, gains.at[0], in_s.at[6]))
    loads.append(pltpu.make_async_copy(gain_b, gains.at[1], in_s.at[7]))
    for c in range(2):
        loads.append(pltpu.make_async_copy(x_ref.at[:, pl.ds(c * STREAM, STREAM)], xs_ref.at[0, c, z, y], in_s.at[8 + c]))
    for c in loads:
        c.start()

    def wrap(v, n):
        return lax.rem(v + n, n)

    def to_y(v):
        return {"fs": z * NY + v}

    def to_z(v):
        return {"fs": v * NY + y}

    def to_zz(v):
        return {"gr": v // NZ, "fs": lax.rem(v, NZ) * NY + y}

    def to_x(v):
        return {"tp": v * 2 + core}

    sibling = {"tp": x * 2 + 1 - core}
    y_up, y_down, y_far = wrap(y + 1, NY), wrap(y - 1, NY), wrap(y + 2, NY)
    x_up, x_down, x_far = wrap(x + 1, NX), wrap(x - 1, NX), wrap(x + 2, NX)

    def remote(src, dst, s, r, to):
        return pltpu.make_async_remote_copy(src, dst, s, r, device_id=to, device_id_type=MESH)

    barrier = pltpu.get_barrier_semaphore()

    def greet_z(i, _):
        pl.semaphore_signal(barrier, inc=1, device_id=to_zz(lax.rem(zz + i, NG * NZ)), device_id_type=MESH)
        return 0

    lax.fori_loop(1, NG * NZ, greet_z, 0)

    def to_plane(i):
        return {"fs": z * NY + lax.rem(y + i, NY), "tp": lax.rem(x + i // NY, NX) * 2 + core}

    def greet_plane(i, _):
        pl.semaphore_signal(barrier, inc=1, device_id=to_plane(i), device_id_type=MESH)
        return 0

    lax.fori_loop(1, NX * NY, greet_plane, 0)
    pl.semaphore_signal(barrier, inc=1, device_id=sibling, device_id_type=MESH)

    def pack(h):
        eye = lax.broadcasted_iota(jnp.int32, (32, 32), 0) == lax.broadcasted_iota(jnp.int32, (32, 32), 1)
        gain = jnp.sum(jnp.where(eye, jnp.broadcast_to(gains[h], (32, 32)), 0.0), axis=1, keepdims=True)
        three = [loaded[h * 3] * gain, loaded[h * 3 + 1] * gain, loaded[h * 3 + 2]]
        for at in range(NY):
            for p in range(NX):
                first, count = at * WIDTH + p * PART, min(PART, WIDTH - p * PART)
                pieces = [jnp.pad(v[:, first : first + count], ((0, 0), (0, PART - count))) for v in three]
                wp[h, p * NY + at] = jnp.concatenate(pieces, axis=1).astype(jnp.bfloat16)

    for c in loads:
        c.wait()
    pack(0)
    pack(1)
    for h in range(2):
        r1[h, x, pl.ds(y * 32, 32), :] = wp[h, x * NY + y]
    pl.semaphore_wait(barrier, NG * NZ - 1 + NX * NY - 1 + 1)

    STEPS = 5

    def each(s, f_low, f_high):
        d1 = s + jnp.where(s >= 3, 1, 0)
        fits = (s >= 0) & (s < STEPS)

        @pl.when(fits & (z - d1 >= 0))
        def _():
            f_low(z - d1, d1)

        @pl.when(fits & (d1 > 0) & (z + d1 < NZ))
        def _():
            f_high(z + d1, d1)

        d2 = s + jnp.where(s >= 3, 3, 1)
        second = (s >= 2) & (s < STEPS)

        @pl.when(second & (z - d2 >= 0))
        def _():
            f_low(z - d2, d2)

        @pl.when(second & (z + d2 < NZ))
        def _():
            f_high(z + d2, d2)

    z_up, z_down = jnp.minimum(z + 1, NZ - 1), jnp.maximum(z - 1, 0)
    far = (STRIDE, 2 * STRIDE)

    def up_by(d):
        return to_z(jnp.minimum(z + d, NZ - 1))

    def down_by(d):
        return to_z(jnp.maximum(z - d, 0))

    def chained(d):
        return lax.rem(d, STRIDE) != STRIDE - 1

    def gather_copy(k, c, zs, ys, link, arrival, to):
        blk = xs_ref.at[k, c, zs, ys]
        return remote(blk, blk, ag_s.at[2 * k + c, link], ag_r.at[2 * k + c, arrival], to)

    DIRECT, RELAYED, UPWARD, DOWNWARD = 8, 9, 10, 18

    def even(v):
        return lax.rem(v, 2) == 0

    def arrived(k, c, zs, arrival):
        gather_copy(k, c, zs, y, 0, arrival, to_y(y_up)).wait_recv()

    def along_y(k, c, zs):
        gather_copy(k, c, zs, y, 0, jnp.where(even(zs), zs, DIRECT), to_y(y_up)).start()
        gather_copy(k, c, zs, y, 0, jnp.where(even(zs), DIRECT, zs), to_y(y_down)).start()

    def gather_own(k, c):
        for d in reversed(far):

            @pl.when(z + d < NZ)
            def _():
                gather_copy(k, c, z, y, 1, UPWARD + z, up_by(d)).start()

            @pl.when(z - d >= 0)
            def _():
                gather_copy(k, c, z, y, 1, DOWNWARD + z, down_by(d)).start()

    def gather_low(k, c, zs, d):
        @pl.when(d > 0)
        def _():
            arrived(k, c, zs, UPWARD + zs)

        @pl.when((z < NZ - 1) & chained(d))
        def _():
            gather_copy(k, c, zs, y, 1, UPWARD + zs, to_z(z_up)).start()

        @pl.when((d == 0) & (z > 0))
        def _():
            gather_copy(k, c, zs, y, 1, DOWNWARD + zs, to_z(z_down)).start()

        along_y(k, c, zs)

    def gather_high(k, c, zs, d):
        arrived(k, c, zs, DOWNWARD + zs)

        @pl.when((z > 0) & chained(d))
        def _():
            gather_copy(k, c, zs, y, 1, DOWNWARD + zs, to_z(z_down)).start()

        along_y(k, c, zs)

    def gather_relay(k, c, zs):
        origin = jnp.where(even(zs), y_down, y_up)
        onward = jnp.where(even(zs), y_up, y_down)
        arrived(k, c, zs, zs)
        gather_copy(k, c, zs, origin, 0, RELAYED, to_y(onward)).start()

    LAG = 1

    def gather_tick(k, c, s):
        each(s, lambda zs, d: gather_low(k, c, zs, d), lambda zs, d: gather_high(k, c, zs, d))

        @pl.when(s == 0)
        def _():
            gather_own(k, c)

        each(s - LAG, lambda zs, d: gather_relay(k, c, zs), lambda zs, d: gather_relay(k, c, zs))

    def gather_end(k, c):
        for arrival in (DIRECT, RELAYED):
            blocks = land.at[0, 0, 0]
            remote(blocks, blocks, ag_s.at[2 * k + c, 0], ag_r.at[2 * k + c, arrival], to_y(y_up)).wait_recv()

    def wait_sent(sem, blocks):
        remote(blocks, blocks, sem, ag_r.at[0, 0], to_y(y_up)).wait_send()

    def gather_drain(j):
        wait_sent(ag_s.at[j, 0], land.at[0, 0, 0:3])

        @pl.when((z == 0) | (z == 7))
        def _():
            wait_sent(ag_s.at[j, 1], land.at[0, 0, 0, 0:3])

        @pl.when((z == 2) | (z == 5))
        def _():
            wait_sent(ag_s.at[j, 1], land.at[0, 0, 0, 0:7])

        @pl.when((z == 1) | (z == 3) | (z == 4) | (z == 6))
        def _():
            wait_sent(ag_s.at[j, 1], land.at[0, 0, 0:3, 0:3])

    FAR, UP, DN, ZP, ZM, XP, XM = 0, 1, 2, 3, 4, (5, 6), (7, 8)
    BOTH, CHAIN_UP, CHAIN_DOWN, FAR_UP, FAR_DOWN = 8, 16, 24, (32, 33), (34, 35)

    def send_part(k, c, zd, col, link, kind, arrival, to):
        there = land.at[k, c, kind, zd]
        return remote(part.at[k, c, zd, col], there, rs_s.at[2 * k + c, link], rs_r.at[2 * k + c, arrival], to)

    def landed(k, c, blk, arrival):
        remote(blk, blk, rs_s.at[2 * k + c, 0], rs_r.at[2 * k + c, arrival], to_y(y_up)).wait_recv()

    def wide(v):
        return v.astype(jnp.float32)

    def sum_far(k, c, zd):
        onward = jnp.where(even(zd), y_up, y_down)
        direct = jnp.where(even(zd), y_down, y_up)
        send_part(k, c, zd, y_far, 0, FAR, zd, to_y(onward)).start()
        send_part(k, c, zd, direct, 0, jnp.where(even(zd), DN, UP), BOTH + zd, to_y(direct)).start()

    def sum_near(k, c, zd):
        target = jnp.where(even(zd), y_up, y_down)
        landed(k, c, land.at[k, c, FAR, zd], zd)
        part[k, c, zd, target] = (wide(part[k, c, zd, target]) + wide(land[k, c, FAR, zd])).astype(jnp.bfloat16)
        send_part(k, c, zd, target, 0, jnp.where(even(zd), UP, DN), BOTH + zd, to_y(target)).start()

    def column_sum(k, c, zd):
        landed(k, c, land.at[k, c, UP, 0:2], BOTH + zd)
        return wide(part[k, c, zd, y]) + wide(land[k, c, UP, zd]) + wide(land[k, c, DN, zd])

    def sum_along_z(k, c, zd, d, chain, arrival, express, far_arrival, more, to_next, by):
        own = column_sum(k, c, zd)
        joined = more & chained(d)

        @pl.when(jnp.logical_not(joined))
        def _():
            part[k, c, zd, y] = own.astype(jnp.bfloat16)

        @pl.when(joined)
        def _():
            landed(k, c, land.at[k, c, chain, zd], arrival + zd)
            part[k, c, zd, y] = (own + wide(land[k, c, chain, zd])).astype(jnp.bfloat16)

        @pl.when(lax.rem(d, STRIDE) != 0)
        def _():
            send_part(k, c, zd, y, 1, chain, arrival + zd, to_next).start()

        for i in range(2):

            @pl.when(d == far[i])
            def _():
                send_part(k, c, zd, y, 1, express[i], far_arrival[i], by(far[i])).start()

    def sum_upward(k, c, zd, d):
        sum_along_z(k, c, zd, d, ZP, CHAIN_UP, XP, FAR_UP, z > 0, to_z(z_up), up_by)

    def sum_downward(k, c, zd, d):
        @pl.when(d > 0)
        def _():
            sum_along_z(k, c, zd, d, ZM, CHAIN_DOWN, XM, FAR_DOWN, z < NZ - 1, to_z(z_down), down_by)

    def partial_sum(k, c, zd):
        w = wh[3 * k + 2, 0:WIDTH, pl.ds(pl.multiple_of(zd * 256, 256), 256)]
        p = lax.dot_general(w, hid[c], (((0,), (0,)), ((), ())), preferred_element_type=jnp.float32)
        part[k, c, zd] = p.astype(jnp.bfloat16).reshape(NY, FEAT, STREAM)

    def sum_tick(k, c, i):
        s = STEPS - 1 - i

        def start(zd, d):
            partial_sum(k, c, zd)
            sum_far(k, c, zd)

        each(s, start, start)
        each(s + 1, lambda zd, d: sum_near(k, c, zd), lambda zd, d: sum_near(k, c, zd))
        each(s + 2, lambda zd, d: sum_downward(k, c, zd, d), lambda zd, d: sum_upward(k, c, zd, d))

    def sum_end(k, c):
        total = column_sum(k, c, z)
        for kind, there, arrival in (
            (ZP, z > 0, CHAIN_UP + z),
            (ZM, z < NZ - 1, CHAIN_DOWN + z),
            (XP[0], z - far[0] >= 0, FAR_UP[0]),
            (XP[1], z - far[1] >= 0, FAR_UP[1]),
            (XM[0], z + far[0] < NZ, FAR_DOWN[0]),
            (XM[1], z + far[1] < NZ, FAR_DOWN[1]),
        ):

            @pl.when(there)
            def _():
                landed(k, c, land.at[k, c, kind, z], arrival)

            @pl.when(jnp.logical_not(there))
            def _():
                land[k, c, kind, z] = jnp.zeros((FEAT, STREAM), jnp.bfloat16)

            total = total + wide(land[k, c, kind, z])
        value = (wide(xs_ref[k, c, z, y]) + 0.5 * FF ** (-0.5) * total).astype(jnp.bfloat16)

        @pl.when(k == 0)
        def _():
            xs_ref[1, c, z, y] = value

        @pl.when(k == 1)
        def _():
            res_ref[:, pl.ds(pl.multiple_of(c * STREAM, STREAM), STREAM)] = value

    def sum_drain(j):
        wait_sent(rs_s.at[j, 0], land.at[0, 0, 0:3])
        wait_sent(rs_s.at[j, 1], land.at[0, 0, 0, 0:7])

    def w1_start(h):
        def step(i, _):
            at = lax.rem(x + i // NY, NX) * NY + lax.rem(y + i, NY)
            rows = r1.at[h, x, pl.ds(y * 32, 32)]
            remote(wp.at[h, at], rows, w1_s.at[h], w1_r.at[h], to_plane(i)).start()
            return 0

        lax.fori_loop(1, NX * NY, step, 0)

    def w1_wait(h):
        others = wp.at[h, 0 : NX * NY - 1]
        remote(others, others, w1_s.at[h], w1_r.at[h], sibling).wait_recv()

    def turn(h):
        for xs in range(NX):
            r2[h, xs] = r1[h, xs].astype(jnp.float32).T.astype(jnp.bfloat16).reshape(3, PART, 128)

    hub = core == lax.rem(z, 2)

    def part_rows(p):
        return pl.ds(pl.multiple_of(p * PART, 16), PART)

    def w3_columns():
        return pl.ds(pl.multiple_of(zz * 128, 128), 128)

    def w3_start(m):
        def step(i, _):
            target = lax.rem(i, 2) * NZ + (i // 2) * 2 + core

            @pl.when(target == zz)
            def _():
                wh[m, part_rows(x), w3_columns()] = r2[m // 3, i // 2, m % 3]

            @pl.when(target != zz)
            def _():
                block = wh.at[m, part_rows(x), w3_columns()]
                remote(r2.at[m // 3, i // 2, m % 3], block, w3_s.at[m // 3], w3_r.at[m], to_zz(target)).start()

            return 0

        lax.fori_loop(0, 2 * NX, step, 0)

    def w3_drain(h):
        @pl.when(hub)
        def _():
            wait_sent(w3_s.at[h], wh.at[0, 0 : 3 * PART, 0 : 7 * 128])

        @pl.when(jnp.logical_not(hub))
        def _():
            wait_sent(w3_s.at[h], wh.at[0, 0 : 3 * PART, 0 : 8 * 128])

    def w4_copy(m, kind, p, g, to):
        blk = wh.at[m, part_rows(p), pl.ds(g * GCOL, GCOL)]
        return remote(blk, blk, w4_s.at[0], w4_r.at[m, 4 if kind == 2 else 2 * kind + g], to)

    def w5_copy(m, p):
        blk = wh.at[m, part_rows(p)]
        return remote(blk, blk, w5_s.at[0], w5_r.at[m], sibling)

    def w4_send(m):
        @pl.when(hub)
        def _():
            others = wh.at[m, 0:PART, 0 : 15 * 128]
            remote(others, others, w3_s.at[0], w3_r.at[m], sibling).wait_recv()
            for g in range(NGRP):
                w4_copy(m, 0, x, g, to_x(x_up)).start()
                w4_copy(m, 1, x, g, to_x(x_down)).start()
            w5_copy(m, x).start()

    def w4_relay(m):
        @pl.when(hub)
        def _():
            for g in range(NGRP):
                w4_copy(m, 0, x_down, g, to_x(x_up)).wait_recv()
                if g % 2 == 0:
                    w4_copy(m, 2, x_down, g, to_x(x_up)).start()
                w4_copy(m, 1, x_up, g, to_x(x_down)).wait_recv()
                if g % 2 == 1:
                    w4_copy(m, 2, x_up, g, to_x(x_down)).start()
            w5_copy(m, x_down).start()
            w5_copy(m, x_up).start()

    def w5_send(m):
        @pl.when(hub)
        def _():
            far = wh.at[m, part_rows(x_far)]
            remote(far, far, w4_s.at[0], w4_r.at[m, 4], sibling).wait_recv()
            w5_copy(m, x_far).start()

    def w5_wait(m):
        @pl.when(jnp.logical_not(hub))
        def _():
            remote(wh.at[m], wh.at[m], w5_s.at[0], w5_r.at[m], sibling).wait_recv()

    def w_drain():
        for h in range(2):
            wait_sent(w1_s.at[h], wp.at[h, 0 : NX * NY - 1])
            w3_drain(h)

        @pl.when(hub)
        def _():
            wait_sent(w4_s.at[0], wh.at[:, 0 : 3 * PART])
            wait_sent(w5_s.at[0], wh)

    def out_copy(m):
        return pltpu.make_async_copy(wh.at[m, pl.ds(0, WIDTH)], outs[m], out_s.at[m])

    def hidden_units(k, c):
        whole = xs_ref[k, c].reshape(D, STREAM)
        wide_whole = wide(whole)
        squares = jnp.sum(wide_whole * wide_whole, axis=0, keepdims=True)
        row_scale = lax.rsqrt(squares / D + norm_eps) * D ** (-0.5)
        g = jnp.dot(wh[3 * k, 0:WIDTH], whole, preferred_element_type=jnp.float32) * row_scale
        u = jnp.dot(wh[3 * k + 1, 0:WIDTH], whole, preferred_element_type=jnp.float32) * row_scale
        hid[c] = (g / (1.0 + jnp.exp(-g)) * u).astype(jnp.bfloat16)

    def both_streams(f):
        def step(c, _):
            f(c)
            return 0

        lax.fori_loop(0, 2, step, 0)

    def gather_rounds(first, last):
        def step(s, _):
            both_streams(lambda c: gather_tick(0, c, s))
            return 0

        lax.fori_loop(first, last, step, 0)

    w1_start(0)
    gather_rounds(0, 1)
    w1_wait(0)
    turn(0)
    for m in range(3):
        w3_start(m)
    gather_rounds(1, 2)
    w4_send(0)
    w1_start(1)
    gather_rounds(2, 3)
    w4_send(1)
    w4_relay(0)
    gather_rounds(3, 4)
    w4_send(2)
    w4_relay(1)
    w5_send(0)
    gather_rounds(4, 5)
    w4_relay(2)
    w5_send(1)
    gather_rounds(5, STEPS + LAG)
    w1_wait(1)
    turn(1)
    both_streams(lambda c: gather_end(0, c))
    w5_send(2)
    for m in range(3, 6):
        w3_start(m)
    for m in range(2):
        w5_wait(m)
    both_streams(lambda c: hidden_units(0, c))
    w5_wait(2)
    for m in range(3):
        out_copy(m).start()

    SUM = STEPS + 1
    GATHER = SUM + 1
    TURN = GATHER + STEPS + LAG
    AGAIN = TURN + 1
    LAST = AGAIN + SUM

    def tick(n, c):
        t = n - OFFSET * c

        @pl.when(((t >= 0) & (t < SUM)) | ((t >= AGAIN) & (t < LAST)))
        def _():
            k = jnp.where(t >= AGAIN, 1, 0)
            sum_tick(k, c, t - AGAIN * k)

        @pl.when((t == SUM) | (t == LAST))
        def _():
            sum_end(jnp.where(t == LAST, 1, 0), c)

        @pl.when((t >= GATHER) & (t < TURN))
        def _():
            gather_tick(1, c, t - GATHER)

        @pl.when(t == TURN)
        def _():
            gather_end(1, c)

            @pl.when(c == 0)
            def _():
                for m in range(3, 6):
                    w5_wait(m)
                for m in range(3, 6):
                    out_copy(m).start()

            hidden_units(1, c)

    def run(n, _):
        for at, act in ((SUM, w4_send), (GATHER + 2, w4_relay), (GATHER + 5, w5_send)):

            @pl.when(n == at)
            def _():
                for m in range(3, 6):
                    act(m)

        both_streams(lambda c: tick(n, c))
        return 0

    lax.fori_loop(0, LAST + OFFSET + 1, run, 0)

    w_drain()
    for m in range(6):
        out_copy(m).wait()
    for j in range(4):
        gather_drain(j)
        sum_drain(j)


def write_out(*refs):
    ins, outs, held, sems = refs[:7], refs[7:14], refs[14:21], refs[21]
    loads = [pltpu.make_async_copy(ins[i], held[i], sems.at[0, i]) for i in range(7)]
    stores = [pltpu.make_async_copy(held[i], outs[i], sems.at[1, i]) for i in range(7)]
    for c in loads:
        c.start()
    for i in range(7):
        loads[i].wait()
        stores[i].start()
    for c in stores:
        c.wait()


def local(prompt, gain_pre, gate_pre, up_pre, down_pre, gain_post, gate_post, up_post, down_post):
    vm = pl.BlockSpec(memory_space=pltpu.VMEM)
    dma = pltpu.SemaphoreType.DMA
    bf = jnp.bfloat16
    hbm = pl.BlockSpec(memory_space=pltpu.HBM)
    shapes = (jax.ShapeDtypeStruct((FEAT, TOK), bf),) + (jax.ShapeDtypeStruct((WIDTH, D), bf),) * 6
    made = pl.pallas_call(
        kernel,
        out_shape=shapes,
        in_specs=[hbm] * 9,
        out_specs=(vm,) + (hbm,) * 6,
        scratch_shapes=[
            pltpu.VMEM((2, 2, NZ, NY, FEAT, STREAM), bf),
            pltpu.VMEM((2, 2, NZ, NY, FEAT, STREAM), bf),
            pltpu.VMEM((2, 2, 9, NZ, FEAT, STREAM), bf),
            pltpu.VMEM((2, NX * NY, 32, 3 * PART), bf),
            pltpu.VMEM((2, NX, 128, 3 * PART), bf),
            pltpu.VMEM((2, NX, 3, PART, 128), bf),
            pltpu.VMEM((6, ROWS, D), bf),
            pltpu.VMEM((2, 1, 32), jnp.float32),
            pltpu.VMEM((6, 32, NY * WIDTH), jnp.float32),
            pltpu.VMEM((2, WIDTH, STREAM), bf),
            dma((4, 2)),
            dma((4, 26)),
            dma((4, 2)),
            dma((4, 36)),
            dma((2,)),
            dma((2,)),
            dma((2,)),
            dma((6,)),
            dma((1,)),
            dma((6, 5)),
            dma((1,)),
            dma((6,)),
            dma((10,)),
            dma((6,)),
        ],
        compiler_params=pltpu.CompilerParams(
            collective_id=0, has_side_effects=True, vmem_limit_bytes=58 * 1024 * 1024
        ),
    )(
        prompt.T,
        gain_pre.reshape(1, 32),
        gain_post.reshape(1, 32),
        gate_pre,
        up_pre,
        down_pre,
        gate_post,
        up_post,
        down_post,
    )
    res, *served = pl.pallas_call(
        write_out,
        out_shape=shapes,
        in_specs=[hbm] * 7,
        out_specs=(hbm,) * 7,
        scratch_shapes=[pltpu.VMEM(a.shape, bf) for a in shapes] + [dma((2, 7))],
    )(*made)
    return (res.T, *served)


def solution(mesh):
    rows = P(("gr", "fs"))
    block = P(("gr", "fs"), "tp")
    tokens = P(("gr", "tp"), "fs")
    return jax.shard_map(
        local,
        mesh=mesh,
        in_specs=(tokens, rows, block, block, block, rows, block, block, block),
        out_specs=(tokens,) + (P("fs", None),) * 6,
        check_vma=False,
    )
```

time: 151 us -> 141 us (0.934)
  Pallas kernels: 149 us -> 140 us
    pallas_call x1, Pallas kernels: 145 us -> 137 us  [local(): pl.pallas_call(kernel, out_shape=shapes, in_specs=[hbm] * 9, out_specs=(v...]
where the time goes in v5:
time: 141 us
  Pallas kernels  140 us (99%)
    pallas_call x1, Pallas kernels, local(): pl.pallas_call(kernel, out_shape=shapes, in_specs=[hbm] * 9, out_specs=(v...  137 us
    pallas_call x1, Pallas kernels, local(): pl.pallas_call(write_out, out_shape=shapes, in_specs=[hbm] * 7, out_specs...  3.71 us

profile of v5, /device:TPU:6, one launch (start us, length us, event | category | flops | bytes accessed | tf_op | source)
XLA Modules:
  0.0 140.9 jit_solution(9675661150340838356)
XLA Ops:
  0.6 136.6 %shard_map.144 = (bf16[64,512]{1,0:T(8,128)(2,1)}, bf16[176,2048]{1,0:T(8,128)(2,1)}, bf16[176,2048]{1,0:T(8,128)(2,1)}, bf16[176,2048]{1,0:T(8,128)(2,1)}, bf16...) custom-call(bf16[64,512]{1,0:T(8,128)(2,1)} %bitcast.4, f32[1,32]{1,0:T(1,128)} %bitcast.5, ...), custom_call_target="tpu_custom_call" | custom-call | tf_op jit(solution)/shard_map/pallas_call | solution.py:580
  137.2 3.7 %shard_map.145 = (bf16[64,512]{1,0:T(8,128)(2,1)}, bf16[176,2048]{1,0:T(8,128)(2,1)}, bf16[176,2048]{1,0:T(8,128)(2,1)}, bf16[176,2048]{1,0:T(8,128)(2,1)}, bf16...) custom-call(bf16[64,512]{1,0:T(8,128)(2,1)} %get-tuple-element.21.refs_0_, ...), custom_call_target="tpu_custom_call" | custom-call | tf_op jit(solution)/shard_map/pallas_call | solution.py:625

commit v6 on v5

--- a/solution.py
+++ b/solution.py
@@ -140,9 +140,9 @@
 
     def gather_copy(k, c, zs, ys, link, arrival, to):
         blk = xs_ref.at[k, c, zs, ys]
-        return remote(blk, blk, ag_s.at[2 * k + c, link], ag_r.at[2 * k + c, arrival], to)
-
-    DIRECT, RELAYED, UPWARD, DOWNWARD = 8, 9, 10, 18
+        return remote(blk, blk, ag_s.at[2 * k + c, link], ag_r.at[c, arrival], to)
+
+    DIRECT, RELAYED, UPWARD, DOWNWARD = 8, 9, 10, 10
 
     def even(v):
         return lax.rem(v, 2) == 0
@@ -209,7 +209,7 @@
     def gather_end(k, c):
         for arrival in (DIRECT, RELAYED):
             blocks = land.at[0, 0, 0]
-            remote(blocks, blocks, ag_s.at[2 * k + c, 0], ag_r.at[2 * k + c, arrival], to_y(y_up)).wait_recv()
+            remote(blocks, blocks, ag_s.at[2 * k + c, 0], ag_r.at[c, arrival], to_y(y_up)).wait_recv()
 
     def wait_sent(sem, blocks):
         remote(blocks, blocks, sem, ag_r.at[0, 0], to_y(y_up)).wait_send()
@@ -234,10 +234,10 @@
 
     def send_part(k, c, zd, col, link, kind, arrival, to):
         there = land.at[k, c, kind, zd]
-        return remote(part.at[k, c, zd, col], there, rs_s.at[2 * k + c, link], rs_r.at[2 * k + c, arrival], to)
+        return remote(part.at[k, c, zd, col], there, rs_s.at[2 * k + c, link], rs_r.at[c, arrival], to)
 
     def landed(k, c, blk, arrival):
-        remote(blk, blk, rs_s.at[2 * k + c, 0], rs_r.at[2 * k + c, arrival], to_y(y_up)).wait_recv()
+        remote(blk, blk, rs_s.at[2 * k + c, 0], rs_r.at[c, arrival], to_y(y_up)).wait_recv()
 
     def wide(v):
         return v.astype(jnp.float32)
@@ -475,9 +475,9 @@
     turn(0)
     for m in range(3):
         w3_start(m)
+    w1_start(1)
     gather_rounds(1, 2)
     w4_send(0)
-    w1_start(1)
     gather_rounds(2, 3)
     w4_send(1)
     w4_relay(0)
@@ -488,13 +488,13 @@
     gather_rounds(4, 5)
     w4_relay(2)
     w5_send(1)
-    gather_rounds(5, STEPS + LAG)
     w1_wait(1)
     turn(1)
+    for m in range(3, 6):
+        w3_start(m)
+    gather_rounds(5, STEPS + LAG)
     both_streams(lambda c: gather_end(0, c))
     w5_send(2)
-    for m in range(3, 6):
-        w3_start(m)
     for m in range(2):
         w5_wait(m)
     both_streams(lambda c: hidden_units(0, c))
@@ -594,9 +594,9 @@
             pltpu.VMEM((6, 32, NY * WIDTH), jnp.float32),
             pltpu.VMEM((2, WIDTH, STREAM), bf),
             dma((4, 2)),
-            dma((4, 26)),
+            dma((2, 18)),
             dma((4, 2)),
-            dma((4, 36)),
+            dma((2, 36)),
             dma((2,)),
             dma((2,)),
             dma((2,)),

time: 141 us -> 140 us (level)
  Pallas kernels: 140 us -> 138 us
    pallas_call x1, Pallas kernels: 137 us -> 135 us  [local(): pl.pallas_call(kernel, out_shape=shapes, in_specs=[hbm] * 9, out_specs=(v...]
where the time goes in v6:
time: 140 us; the launch traced here: 139 us
  Pallas kernels  138 us (99%)
    pallas_call x1, Pallas kernels, local(): pl.pallas_call(kernel, out_shape=shapes, in_specs=[hbm] * 9, out_specs=(v...  135 us
    pallas_call x1, Pallas kernels, local(): pl.pallas_call(write_out, out_shape=shapes, in_specs=[hbm] * 7, out_specs...  3.71 us

profile of v6, /device:TPU:6, one launch (start us, length us, event | category | flops | bytes accessed | tf_op | source)
XLA Modules:
  0.0 139.1 jit_solution(16844455202204023790)
XLA Ops:
  0.6 134.8 %shard_map.144 = (bf16[64,512]{1,0:T(8,128)(2,1)}, bf16[176,2048]{1,0:T(8,128)(2,1)}, bf16[176,2048]{1,0:T(8,128)(2,1)}, bf16[176,2048]{1,0:T(8,128)(2,1)}, bf16...) custom-call(bf16[64,512]{1,0:T(8,128)(2,1)} %bitcast.4, f32[1,32]{1,0:T(1,128)} %bitcast.5, ...), custom_call_target="tpu_custom_call" | custom-call | tf_op jit(solution)/shard_map/pallas_call | solution.py:580
  135.4 3.7 %shard_map.145 = (bf16[64,512]{1,0:T(8,128)(2,1)}, bf16[176,2048]{1,0:T(8,128)(2,1)}, bf16[176,2048]{1,0:T(8,128)(2,1)}, bf16[176,2048]{1,0:T(8,128)(2,1)}, bf16...) custom-call(bf16[64,512]{1,0:T(8,128)(2,1)} %get-tuple-element.21.refs_0_, ...), custom_call_target="tpu_custom_call" | custom-call | tf_op jit(solution)/shard_map/pallas_call | solution.py:625
